TPU v7x, 128 devices: a whole 4x4x4 slice. The times are simulated.
128 devices in a mesh: sp: 32 (over z, y, core), tp: 4 (over x).
Axes of the slice: x: 4, y: 4, z: 4, core: 2. Of those that a mesh axis runs over, the one named last changes fastest.
Arguments:
- out_grad: bfloat16 [4096, 2048], P('sp', 'tp'), may hold values from -6 to 6
- route_ids: int32 [4096, 2], P('sp'), may hold values from 0 to 31, as said below
- route_weight: float32 [4096, 2], P('sp'), may hold values from 0.1 to 0.9
- expert_inputs: bfloat16 [32, 512, 2048], P('sp'), may hold values from -6 to 6
- gate_weight: bfloat16 [32, 2048, 3072], P('sp', None, 'tp'), may hold values from -0.125 to 0.125
- up_weight: bfloat16 [32, 2048, 3072], P('sp', None, 'tp'), may hold values from -0.125 to 0.125
- down_weight: bfloat16 [32, 3072, 2048], P('sp', 'tp'), may hold values from -0.109375 to 0.109375
- out_gate: bfloat16 [4096, 2048], P('sp', 'tp'), may hold values from -6 to 6
- in_gate: bfloat16 [4096, 2048], P('sp', 'tp'), may hold values from -6 to 6
- values: bfloat16 [4096, 2048], P('sp', 'tp'), may hold values from -6 to 6
- conv_out: bfloat16 [4096, 2048], P('sp', 'tp'), may hold values from -6 to 6
- conv_taps: bfloat16 [3, 2048], P(None, 'tp'), may hold values from -3.5 to 3.5
- proj_weight: bfloat16 [2048, 2048], P(None, 'tp'), may hold values from -0.125 to 0.125
Outputs:
- resid_grad: bfloat16 [4096, 2048], P('sp', 'tp')
- out_gate_grad: bfloat16 [4096, 2048], P('sp', 'tp')
- in_gate_grad: bfloat16 [4096, 2048], P('sp', 'tp')
- values_grad: bfloat16 [4096, 2048], P('sp', 'tp')
- proj_grad: float32 [2048, 2048], P('sp', 'tp')
- gate_grad: bfloat16 [32, 2048, 3072], P('sp', None, 'tp')
- up_grad: bfloat16 [32, 2048, 3072], P('sp', None, 'tp')
- down_grad: bfloat16 [32, 3072, 2048], P('sp', 'tp')
Inputs may be any that keep to these rules, and one draw needn't show every extreme that they name: `route_ids`: each row names two different experts. Among the rows of one device (aligned blocks of 128 rows) no expert is named more than 16 times, and in every draw one expert is named exactly 16 times in every block.
All inputs are finite; a program needn't handle non-finite values.
Results may differ from a plain program's by a relative error of at most 0.017.
Values may be sent and summed in bfloat16 or wider, within the bound.
A program may use at most 128 MiB of HBM per device.

v0:
```python
import math

import jax
import jax.numpy as jnp
from jax import lax
from jax.sharding import Mesh
from jax.sharding import PartitionSpec as P

SP = ("sp_0", "sp_1", "sp_2")


def in_order(pieces, dim):
    lengths = list(pieces.shape[1:])
    lengths[dim] *= pieces.shape[0]
    return jnp.moveaxis(pieces, 0, dim).reshape(lengths)


def sent_to_all(x, axis):
    devices = lax.axis_size(axis)
    return lax.all_to_all(jnp.broadcast_to(x[None], (devices, *x.shape)), axis, 0, 0, tiled=True)


def gathered_copies(x, axis, dim):
    return in_order(sent_to_all(x, axis), dim)


def cut_along(x, dim, devices):
    lengths = x.shape
    pieces = x.reshape(*lengths[:dim], devices, lengths[dim] // devices, *lengths[dim + 1 :])
    return jnp.moveaxis(pieces, dim, 0)


def sum_at_owner(x, axis, dim):
    devices = lax.axis_size(axis)
    pieces = lax.all_to_all(cut_along(x, dim, devices), axis, 0, 0, tiled=True)
    return jnp.sum(pieces.astype(jnp.float32), axis=0)


def turned_blocks(pieces, axes, order):
    lengths = [lax.axis_size(a) for a in axes]
    pieces = pieces.reshape(*lengths, *pieces.shape[1:])
    for k in order:
        pieces = lax.all_to_all(pieces, axes[k], split_axis=k, concat_axis=k, tiled=True)
    return pieces.reshape(-1, *pieces.shape[len(axes) :])


def two_step_exchange(x, groups, order, split_dim, concat_dim):
    devices = lax.axis_size(groups[0]) * lax.axis_size(groups[1])
    pieces = cut_along(x, split_dim, devices)
    return in_order(turned_blocks(pieces, groups, order), concat_dim)


def extended(x, sides, width):
    for axis, dim in sides:
        devices, length = (lax.axis_size(axis), x.shape[dim])
        up = [(i, (i + 1) % devices) for i in range(devices - 1)]
        down = [(j, i) for i, j in up]
        last = lax.slice_in_dim(x, length - width, length, axis=dim)
        first = lax.slice_in_dim(x, 0, width, axis=dim)
        before = lax.ppermute(last, axis, up)
        after = lax.ppermute(first, axis, down)
        x = jnp.concatenate([before, x, after], axis=dim)
    return x


def sum_by_axis(x, axes, dim):
    far, near = axes
    own = sum_at_owner(cut_along(x, dim, lax.axis_size(far)), near, dim + 1)
    return jnp.sum(
        lax.all_to_all(own.astype(jnp.bfloat16), far, 0, 0, tiled=True).astype(jnp.float32), axis=0
    )


def contract_first(left, right):
    return lax.dot_general(
        left, right, (((0,), (0,)), ((), ())), preferred_element_type=jnp.float32
    )


def contract_last(left, right):
    return lax.dot_general(
        left, right, (((1,), (1,)), ((), ())), preferred_element_type=jnp.float32
    )


def expert_backward(inputs, routed, gate_w, up_w, down_w):
    pre_gate = jnp.dot(inputs, gate_w, preferred_element_type=jnp.float32)
    pre_up = jnp.dot(inputs, up_w, preferred_element_type=jnp.float32)
    sigmoid_g = jax.nn.sigmoid(pre_gate)
    activated = pre_gate * sigmoid_g
    hidden = (activated * pre_up).astype(jnp.bfloat16)
    d_hidden = contract_last(routed, down_w)
    d_gate = (d_hidden * pre_up * sigmoid_g * (1.0 + pre_gate * (1.0 - sigmoid_g))).astype(
        jnp.bfloat16
    )
    d_up = (d_hidden * activated).astype(jnp.bfloat16)
    partial_value = contract_last(d_gate, gate_w) + contract_last(d_up, up_w)
    grad_set = (
        contract_first(inputs, d_gate),
        contract_first(inputs, d_up),
        contract_first(hidden, routed),
    )
    return (partial_value, grad_set)


def expert_pass(outgoing, input_rows, gate_weight, up_weight, down_weight):
    arrived = lax.all_to_all(outgoing, SP, split_axis=0, concat_axis=1, tiled=True)
    routed = gathered_copies(arrived, "tp", 2)
    partial_value, grad_set = expert_backward(
        input_rows[0], routed[0], gate_weight[0], up_weight[0], down_weight[0]
    )
    partials = [partial_value]
    gate_list = [grad_set[0]]
    up_list = [grad_set[1]]
    down_list = [grad_set[2]]
    summed = sum_at_owner(jnp.stack(partials).astype(jnp.bfloat16), "tp", 2)
    returned = two_step_exchange(
        summed.astype(jnp.bfloat16), (("sp_0", "sp_1"), "sp_2"), (1, 0), 1, 0
    )
    return (returned, (jnp.stack(gate_list), jnp.stack(up_list), jnp.stack(down_list)))


def per_device(
    out_grad,
    route_ids,
    route_weight,
    expert_inputs,
    gate_weight,
    up_weight,
    down_weight,
    out_gate,
    in_gate,
    values,
    conv_out,
    conv_taps,
    proj_weight,
):
    sp_devices = lax.axis_size(SP)
    tok_rows = out_grad.shape[0]
    local_experts = gate_weight.shape[0]
    all_experts = sp_devices * local_experts
    capacity = 4 * tok_rows // all_experts
    flat_ids = route_ids.reshape(-1)
    onehot = (flat_ids[:, None] == jnp.arange(all_experts, dtype=jnp.int32)[None, :]).astype(
        jnp.int32
    )
    ranked = jnp.sum((jnp.cumsum(onehot, axis=0) - onehot) * onehot, axis=1)
    slot_ids = flat_ids * capacity + ranked
    dispatch = (
        jnp.arange(all_experts * capacity, dtype=jnp.int32)[:, None] == slot_ids[None, :]
    ).astype(jnp.bfloat16)
    weighted = (
        (route_weight[:, :, None] * out_grad.astype(jnp.float32)[:, None, :])
        .astype(jnp.bfloat16)
        .reshape(2 * tok_rows, -1)
    )
    outgoing = jnp.dot(dispatch, weighted, preferred_element_type=jnp.float32).astype(jnp.bfloat16)
    outgoing = outgoing.reshape(all_experts, capacity, -1)
    returned, totals = expert_pass(outgoing, expert_inputs, gate_weight, up_weight, down_weight)
    slot_scale = 1.0 / math.sqrt(expert_inputs.shape[1])
    gate_grad = (totals[0] * slot_scale).astype(jnp.bfloat16)
    up_grad = (totals[1] * slot_scale).astype(jnp.bfloat16)
    down_grad = (totals[2] * slot_scale).astype(jnp.bfloat16)
    combiner = jnp.sum(dispatch.reshape(all_experts * capacity, tok_rows, 2), axis=2)
    moe_part = contract_first(combiner, returned.reshape(all_experts * capacity, -1))
    resid_grad = (out_grad.astype(jnp.float32) + moe_part).astype(jnp.bfloat16)
    resid_full = lax.all_gather(resid_grad, "tp", axis=1, tiled=True)
    mix_grad = jnp.dot(resid_full, proj_weight, preferred_element_type=jnp.float32)
    gate_vals = out_gate.astype(jnp.float32)
    conv_vals = conv_out.astype(jnp.float32)
    mixed_in = (gate_vals * conv_vals).astype(jnp.bfloat16)
    out_gate_grad = (mix_grad * conv_vals).astype(jnp.bfloat16)
    conv_grad = (mix_grad * gate_vals).astype(jnp.bfloat16)
    padded = extended(conv_grad, ((SP, 0),), 1).astype(jnp.float32)
    tap_vals = conv_taps.astype(jnp.float32)
    value_grad = padded[2:] * tap_vals[0] + padded[1:-1] * tap_vals[1] + padded[:-2] * tap_vals[2]
    in_gate_grad = (value_grad * values.astype(jnp.float32)).astype(jnp.bfloat16)
    values_grad = (value_grad * in_gate.astype(jnp.float32)).astype(jnp.bfloat16)
    token_scale = 1.0 / math.sqrt(tok_rows * sp_devices)
    proj_sum = sum_by_axis(
        contract_first(resid_full, mixed_in).astype(jnp.bfloat16), (("sp_0", "sp_1"), "sp_2"), 0
    )
    proj_grad = proj_sum * token_scale
    return (
        resid_grad,
        out_gate_grad,
        in_gate_grad,
        values_grad,
        proj_grad,
        gate_grad,
        up_grad,
        down_grad,
    )


def solution(mesh):
    split = Mesh(mesh.devices.reshape(4, 4, 2, mesh.shape["tp"]), ("sp_0", "sp_1", "sp_2", "tp"))
    return jax.shard_map(
        per_device,
        mesh=split,
        in_specs=(
            P(SP, "tp"),
            P(SP, None),
            P(SP, None),
            P(SP, None, None),
            P(SP, None, "tp"),
            P(SP, None, "tp"),
            P(SP, "tp", None),
            P(SP, "tp"),
            P(SP, "tp"),
            P(SP, "tp"),
            P(SP, "tp"),
            P(None, "tp"),
            P(None, "tp"),
        ),
        out_specs=(
            P(SP, "tp"),
            P(SP, "tp"),
            P(SP, "tp"),
            P(SP, "tp"),
            P(SP, "tp"),
            P(SP, None, "tp"),
            P(SP, None, "tp"),
            P(SP, "tp", None),
        ),
        check_vma=False,
    )
```

profile of v0, /device:TPU:0, one launch (start us, length us, event | category | flops | bytes accessed | tf_op | source)
XLA Modules:
  0.0 187.3 jit_solution(11504658302749847632)
XLA Ops:
  0.6 0.9 copy.75
  1.9 0.6 reduce-window.6
  2.8 1.8 mul.130
  4.7 2.2 %mul.131 = f32[256,512]{1,0:T(8,128)} reshape(f32[128,2,512]{2,1,0:T(2,128)} %mul.130) | data formatting | bytes 1048576 | tf_op jit(solution)/shard_map/mul | solution.py:153
  6.8 0.8 copy.79
  7.8 1.4 convolution_convert_fusion.1
  9.2 19.9 %all_to_all.39 = bf16[32,16,512]{2,1,0:T(8,128)(2,1)} all-to-all(bf16[32,16,512]{2,1,0:T(8,128)(2,1)S(1)} %bitcast.89), channel_id=1, replica_groups=mesh['sp_0'=4,'sp_1'=4,'sp_2'=2,'tp'=4] {'sp_0','sp_1','sp_2'}, dimensions={0} | all-to-all | bytes 1048576 | tf_op jit(solution)/shard_map/all_to_all | solution.py:107
  29.1 2.0 %copy.80 = bf16[512,512]{0,1:T(8,128)(2,1)} copy(bf16[512,512]{1,0:T(8,128)(2,1)} %bitcast.90) | data formatting | bytes 1048576 | tf_op jit(solution)/shard_map/broadcast_in_dim | solution.py:20
  31.2 2.5 %broadcast_in_dim.5 = bf16[4,1,512,512]{2,3,1,0:T(8,128)(2,1)} broadcast(bf16[512,512]{0,1:T(8,128)(2,1)} %copy.80), dimensions={2,3} | broadcast | bytes 2621440 | tf_op jit(solution)/shard_map/broadcast_in_dim | solution.py:20
  33.7 4.4 %all-to-all-start.1 = ((bf16[4,1,512,512]{2,3,1,0:T(8,128)(2,1)}), bf16[4,1,512,512]{2,3,1,0:T(8,128)(2,1)}, u32[]{:S(2)}, u32[]{:S(2)}) async-start(bf16[4,1,512,512]{2,3,1,0:T(8,128)(2,1)} %broadcast_in_dim.5), calls=%async_computation.1 | async-start | bytes 4194304 | tf_op jit(solution)/shard_map/all_to_all | solution.py:20
  38.2 4.7 %fusion.2 = f32[512,768]{1,0:T(8,128)} fusion(bf16[1,2048,768]{2,1,0:T(8,128)(2,1)S(1)} %copy-done, bf16[1,512,2048]{2,1,0:T(8,128)(2,1)} %param.16), kind=kOutput, calls=%fused_computation.6 | convolution fusion | flops 1610612736 | bytes 6815744 | tf_op jit(solution)/shard_map/dot_general | solution.py:87
  42.9 2.9 %fusion.6 = f32[512,768]{1,0:T(8,128)} fusion(bf16[1,2048,768]{2,1,0:T(8,128)(2,1)S(1)} %copy-done.12, bf16[1,512,2048]{2,1,0:T(8,128)(2,1)S(1)} %copy-done.14), kind=kOutput, calls=%fused_computation.10 | convolution fusion | flops 1610612736 | bytes 6815744 | tf_op jit(solution)/shard_map/dot_general | solution.py:88
  45.8 19.3 %all-to-all-done.1 = bf16[4,1,512,512]{2,3,1,0:T(8,128)(2,1)} async-done(((bf16[4,1,512,512]{2,3,1,0:T(8,128)(2,1)}), bf16[4,1,512,512]{2,3,1,0:T(8,128)(2,1)}, u32[]{:S(2)}, u32[]{:S(2)}) %all-to-all-start.1) | async-done | bytes 2097184 | tf_op jit(solution)/shard_map/all_to_all | solution.py:20
  65.1 5.6 %multiply_convert_fusion.4 = (bf16[512,768]{1,0:T(8,128)(2,1)S(1)}, bf16[512,768]{1,0:T(8,128)(2,1)S(1)}) fusion(f32[512,768]{1,0:T(8,128)} %fusion.2, f32[512,768]{1,0:T(8,128)} %fusion.6, bf16[512,2048]{0,1:T(8,128)(2,1)} %bitcast.5, bf16[1,768,2048]{2,1,0:T(8,128)(2,1)} %param.19), kind=kOutput, calls=%fused_computation.26 | convolution fusion | flops 1615724544 | bytes 9961472 | tf_op jit(solution)/shard_map/dot_general | solution.py:81
  70.8 1.8 fusion
  72.6 0.6 copy-done.13
  73.2 3.1 %add_convert_fusion = bf16[512,2048]{1,0:T(8,128)(2,1)} fusion(f32[512,2048]{1,0:T(8,128)S(1)} %fusion, bf16[512,768]{1,0:T(8,128)(2,1)S(1)} %get-tuple-element.58, bf16[1,2048,768]{2,1,0:T(8,128)(2,1)S(1)} %copy-done.13), kind=kOutput, calls=%fused_computation.3 | convolution fusion | flops 1612709888 | bytes 10223616 | tf_op jit(solution)/shard_map/dot_general | solution.py:81
  76.4 3.3 %reshape.83 = bf16[1,512,4,512]{3,2,1,0:T(4,128)(2,1)S(1)} reshape(bf16[512,2048]{1,0:T(8,128)(2,1)} %add_convert_fusion) | data formatting | bytes 4194304 | tf_op jit(solution)/shard_map/reshape | solution.py:29
  79.7 1.7 copy.93
  81.4 3.7 %all-to-all-start.2 = ((bf16[4,1,512,512]{3,2,1,0:T(8,128)(2,1)}), bf16[4,1,512,512]{3,2,1,0:T(8,128)(2,1)S(1)}, u32[]{:S(2)}, u32[]{:S(2)}) async-start(bf16[4,1,512,512]{3,2,1,0:T(8,128)(2,1)} %bitcast.85), calls=%async_computation.2 | async-start | bytes 4194304 | tf_op jit(solution)/shard_map/all_to_all | solution.py:35
  85.5 25.7 %all-to-all-done.2 = bf16[4,1,512,512]{3,2,1,0:T(8,128)(2,1)S(1)} async-done(((bf16[4,1,512,512]{3,2,1,0:T(8,128)(2,1)}), bf16[4,1,512,512]{3,2,1,0:T(8,128)(2,1)S(1)}, u32[]{:S(2)}, u32[]{:S(2)}) %all-to-all-start.2) | async-done | bytes 2097184 | tf_op jit(solution)/shard_map/all_to_all | solution.py:35
  111.2 0.6 reduce_sum.59
  111.9 4.3 %all_to_all.40 = bf16[16,2,1,16,512]{4,3,0,2,1:T(8,128)(2,1)S(1)} all-to-all(bf16[16,2,1,16,512]{4,3,0,2,1:T(8,128)(2,1)S(1)} %copy.83), channel_id=1, replica_groups=mesh['sp_0'=4,'sp_1'=4,'sp_2'=2,'tp'=4] {'sp_2'}, dimensions={1} | all-to-all | bytes 1048576 | tf_op jit(solution)/shard_map/all_to_all | solution.py:43
  116.1 0.8 copy.84
  117.0 4.6 %all-to-all-start.4 = ((bf16[16,2,1,16,512]{4,3,1,2,0:T(8,128)(2,1)}), bf16[16,2,1,16,512]{4,3,1,2,0:T(8,128)(2,1)S(1)}, u32[]{:S(2)}, u32[]{:S(2)}) async-start(bf16[16,2,1,16,512]{4,3,1,2,0:T(8,128)(2,1)} %copy.84), calls=%async_computation.4 | async-start | bytes 1048576 | tf_op jit(solution)/shard_map/all_to_all | solution.py:43
  121.6 5.8 %fusion.12 = bf16[1,768,2048]{2,1,0:T(8,128)(2,1)} fusion(bf16[512,2048]{0,1:T(8,128)(2,1)} %bitcast.5, f32[512,768]{1,0:T(8,128)} %fusion.6, f32[512,768]{1,0:T(8,128)S(1)} %copy-done.19), kind=kOutput, calls=%fused_computation.17 | convolution fusion | flops 1616117760 | bytes 8388608 | tf_op jit(solution)/shard_map/dot_general | solution.py:75
  127.4 3.5 %fusion.10 = bf16[1,2048,768]{1,2,0:T(8,128)(2,1)} fusion(bf16[512,768]{1,0:T(8,128)(2,1)S(1)} %copy-done.18, bf16[1,512,2048]{2,1,0:T(8,128)(2,1)S(1)} %copy-done.15), kind=kOutput, calls=%fused_computation.15 | convolution fusion | flops 1613758464 | bytes 6029312 | tf_op jit(solution)/shard_map/dot_general | solution.py:75
  130.9 2.5 %all-to-all-done.4 = bf16[16,2,1,16,512]{4,3,1,2,0:T(8,128)(2,1)S(1)} async-done(((bf16[16,2,1,16,512]{4,3,1,2,0:T(8,128)(2,1)}), bf16[16,2,1,16,512]{4,3,1,2,0:T(8,128)(2,1)S(1)}, u32[]{:S(2)}, u32[]{:S(2)}) %all-to-all-start.4) | async-done | bytes 524320 | tf_op jit(solution)/shard_map/all_to_all | solution.py:43
  133.4 0.3 fusion.20
  133.7 13.4 %all_gather.3 = bf16[128,2048]{1,0:T(8,128)(2,1)S(1)} all-gather(bf16[128,512]{1,0:T(8,128)(2,1)S(1)} %fusion.20), channel_id=1, replica_groups=mesh['sp_0'=4,'sp_1'=4,'sp_2'=2,'tp'=4] {'tp'}, dimensions={1}, use_global_device_ids=true | all-gather | bytes 655360 | tf_op jit(solution)/shard_map/all_gather | solution.py:167
  147.1 0.7 convolution_convert_fusion
  147.8 1.1 fusion.24
  149.0 0.6 fusion.38
  149.6 1.3 collective-permute-start
  150.8 1.3 collective-permute-start.1
  152.1 0.2 copy.92
  152.4 6.9 %all_to_all.41 = bf16[2,16,64,512]{3,2,1,0:T(8,128)(2,1)S(1)} all-to-all(bf16[2,16,64,512]{3,2,1,0:T(8,128)(2,1)S(1)} %bitcast.87), channel_id=1, replica_groups=mesh['sp_0'=4,'sp_1'=4,'sp_2'=2,'tp'=4] {'sp_2'}, dimensions={0} | all-to-all | bytes 4194304 | tf_op jit(solution)/shard_map/all_to_all | solution.py:35
  159.2 1.7 reduce_sum.60
  160.9 6.5 %all-to-all-start.6 = ((bf16[16,64,512]{2,1,0:T(8,128)(2,1)}), bf16[16,64,512]{2,1,0:T(8,128)(2,1)}, u32[]{:S(2)}, u32[]{:S(2)}) async-start(bf16[16,64,512]{2,1,0:T(8,128)(2,1)} %reduce_sum.60), calls=%async_computation.6 | async-start | bytes 2097152 | tf_op jit(solution)/shard_map/all_to_all | solution.py:70
  167.4 5.4 %fusion.11 = bf16[1,2048,768]{1,2,0:T(8,128)(2,1)} fusion(bf16[512,768]{1,0:T(8,128)(2,1)} %copy-done.16, bf16[1,512,2048]{2,1,0:T(8,128)(2,1)} %param.16), kind=kOutput, calls=%fused_computation.16 | convolution fusion | flops 1613758464 | bytes 6029312 | tf_op jit(solution)/shard_map/dot_general | solution.py:75
  172.8 2.8 %copy.86 = bf16[1,2048,768]{2,1,0:T(8,128)(2,1)} copy(bf16[1,2048,768]{1,2,0:T(8,128)(2,1)S(1)} %copy-done.2) | data formatting | bytes 6291456
  175.6 4.8 %copy.87 = bf16[1,2048,768]{2,1,0:T(8,128)(2,1)} copy(bf16[1,2048,768]{1,2,0:T(8,128)(2,1)} %fusion.11) | data formatting | bytes 6291456
  180.4 0.7 maximum_convert_fusion
  181.1 0.8 multiply_convert_fusion.9
  181.9 0.7 multiply_convert_fusion.10
  182.6 2.7 %all-to-all-done.6 = bf16[16,64,512]{2,1,0:T(8,128)(2,1)} async-done(((bf16[16,64,512]{2,1,0:T(8,128)(2,1)}), bf16[16,64,512]{2,1,0:T(8,128)(2,1)}, u32[]{:S(2)}, u32[]{:S(2)}) %all-to-all-start.6) | async-done | bytes 1048608 | tf_op jit(solution)/shard_map/all_to_all | solution.py:70
  185.2 1.4 convert_reduce_fusion
  186.6 0.7 broadcast_multiply_fusion
  (56 shorter events, 1.2 us)
Async XLA Ops:
  0.6 37.5 %copy-start = (bf16[1,2048,768]{2,1,0:T(8,128)(2,1)S(1)}, bf16[1,2048,768]{2,1,0:T(8,128)(2,1)}, u32[]{:S(2)}) copy-start(bf16[1,2048,768]{2,1,0:T(8,128)(2,1)} %param.17) | copy-start | bytes 9437188
  33.7 31.4 %all-to-all-start.1 = ((bf16[4,1,512,512]{2,3,1,0:T(8,128)(2,1)}), bf16[4,1,512,512]{2,3,1,0:T(8,128)(2,1)}, u32[]{:S(2)}, u32[]{:S(2)}) async-start(bf16[4,1,512,512]{2,3,1,0:T(8,128)(2,1)} %broadcast_in_dim.5), calls=%async_computation.1 | async-start | bytes 4194304 | tf_op jit(solution)/shard_map/all_to_all | solution.py:20
  38.2 4.7 %copy-start.12 = (bf16[1,2048,768]{2,1,0:T(8,128)(2,1)S(1)}, bf16[1,2048,768]{2,1,0:T(8,128)(2,1)}, u32[]{:S(2)}) copy-start(bf16[1,2048,768]{2,1,0:T(8,128)(2,1)} %param.18) | copy-start | bytes 9437188
  38.2 4.7 %copy-start.14 = (bf16[1,512,2048]{2,1,0:T(8,128)(2,1)S(1)}, bf16[1,512,2048]{2,1,0:T(8,128)(2,1)}, u32[]{:S(2)}) copy-start(bf16[1,512,2048]{2,1,0:T(8,128)(2,1)} %param.16) | copy-start | bytes 6291460
  70.7 1.9 copy-start.17
  70.8 1.9 copy-start.16
  70.8 2.5 %copy-start.13 = (bf16[1,2048,768]{2,1,0:T(8,128)(2,1)S(1)}, bf16[1,2048,768]{2,1,0:T(8,128)(2,1)}, u32[]{:S(2)}) copy-start(bf16[1,2048,768]{2,1,0:T(8,128)(2,1)} %param.18) | copy-start | bytes 9437188
  81.4 4.0 %copy-start.11 = (s32[128,2]{0,1:T(2,128)S(1)}, s32[128,2]{0,1:T(2,128)}, u32[]{:S(2)}) copy-start(s32[128,2]{0,1:T(2,128)} %param.14) | copy-start | bytes 3076
  81.4 4.1 %copy-start.10 = (bf16[3,512]{1,0:T(4,128)(2,1)S(1)}, bf16[3,512]{1,0:T(4,128)(2,1)}, u32[]{:S(2)}) copy-start(bf16[3,512]{1,0:T(4,128)(2,1)} %param.24) | copy-start | bytes 9220
  81.4 29.7 %all-to-all-start.2 = ((bf16[4,1,512,512]{3,2,1,0:T(8,128)(2,1)}), bf16[4,1,512,512]{3,2,1,0:T(8,128)(2,1)S(1)}, u32[]{:S(2)}, u32[]{:S(2)}) async-start(bf16[4,1,512,512]{3,2,1,0:T(8,128)(2,1)} %bitcast.85), calls=%async_computation.2 | async-start | bytes 4194304 | tf_op jit(solution)/shard_map/all_to_all | solution.py:35
  111.9 9.7 %copy-start.19 = (f32[512,768]{1,0:T(8,128)S(1)}, f32[512,768]{1,0:T(8,128)}, u32[]{:S(2)}) copy-start(f32[512,768]{1,0:T(8,128)} %fusion.2) | copy-start | bytes 4718596
  117.0 16.4 %all-to-all-start.4 = ((bf16[16,2,1,16,512]{4,3,1,2,0:T(8,128)(2,1)}), bf16[16,2,1,16,512]{4,3,1,2,0:T(8,128)(2,1)S(1)}, u32[]{:S(2)}, u32[]{:S(2)}) async-start(bf16[16,2,1,16,512]{4,3,1,2,0:T(8,128)(2,1)} %copy.84), calls=%async_computation.4 | async-start | bytes 1048576 | tf_op jit(solution)/shard_map/all_to_all | solution.py:43
  121.6 5.8 %copy-start.15 = (bf16[1,512,2048]{2,1,0:T(8,128)(2,1)S(1)}, bf16[1,512,2048]{2,1,0:T(8,128)(2,1)}, u32[]{:S(2)}) copy-start(bf16[1,512,2048]{2,1,0:T(8,128)(2,1)} %param.16) | copy-start | bytes 6291460
  121.6 5.8 %copy-start.18 = (bf16[512,768]{1,0:T(8,128)(2,1)S(1)}, bf16[512,768]{1,0:T(8,128)(2,1)}, u32[]{:S(2)}) copy-start(bf16[512,768]{1,0:T(8,128)(2,1)} %copy-done.17) | copy-start | bytes 2359300
  127.4 6.0 %copy-start.4 = (bf16[128,512]{1,0:T(8,128)(2,1)S(1)}, bf16[128,512]{1,0:T(8,128)(2,1)}, u32[]{:S(2)}) copy-start(bf16[128,512]{1,0:T(8,128)(2,1)} %param.13) | copy-start | bytes 393220
  127.4 19.7 %copy-start.5 = (bf16[128,512]{1,0:T(8,128)(2,1)S(1)}, bf16[128,512]{1,0:T(8,128)(2,1)}, u32[]{:S(2)}) copy-start(bf16[128,512]{1,0:T(8,128)(2,1)} %param.20) | copy-start | bytes 393220
  127.4 19.7 %copy-start.6 = (bf16[128,512]{1,0:T(8,128)(2,1)S(1)}, bf16[128,512]{1,0:T(8,128)(2,1)}, u32[]{:S(2)}) copy-start(bf16[128,512]{1,0:T(8,128)(2,1)} %param.23) | copy-start | bytes 393220
  133.4 14.4 %copy-start.3 = (bf16[2048,512]{1,0:T(8,128)(2,1)S(1)}, bf16[2048,512]{1,0:T(8,128)(2,1)}, u32[]{:S(2)}) copy-start(bf16[2048,512]{1,0:T(8,128)(2,1)} %param.25) | copy-start | bytes 6291460
  133.7 15.3 %copy-start.7 = (bf16[128,512]{1,0:T(8,128)(2,1)}, bf16[128,512]{1,0:T(8,128)(2,1)S(1)}, u32[]{:S(2)}) copy-start(bf16[128,512]{1,0:T(8,128)(2,1)S(1)} %fusion.20) | copy-start | bytes 393220
  149.6 30.9 %collective-permute-start = (bf16[1,512]{1,0:T(2,128)(2,1)}, bf16[1,512]{1,0:T(2,128)(2,1)S(1)}, u32[]{:S(2)}, u32[]{:S(2)}) collective-permute-start(bf16[1,512]{1,0:T(2,128)(2,1)} %get-tuple-element.62), channel_id=1, source_target_pairs={{0,4},{4,8},{8,12},{12,16},{16,20},{20,24},{24,28},{28,32},{32,36}... | collective-permute-start | bytes 3080 | tf_op jit(solution)/shard_map/ppermute | solution.py:60
  150.8 29.6 %collective-permute-start.1 = (bf16[1,512]{1,0:T(2,128)(2,1)}, bf16[1,512]{1,0:T(2,128)(2,1)}, u32[]{:S(2)}, u32[]{:S(2)}) collective-permute-start(bf16[1,512]{1,0:T(2,128)(2,1)} %get-tuple-element.63), channel_id=1, source_target_pairs={{4,0},{8,4},{12,8},{16,12},{20,16},{24,20},{28,24},{32,28},{36,32}... | collective-permute-start | bytes 3080 | tf_op jit(solution)/shard_map/ppermute | solution.py:61
  160.9 24.4 %all-to-all-start.6 = ((bf16[16,64,512]{2,1,0:T(8,128)(2,1)}), bf16[16,64,512]{2,1,0:T(8,128)(2,1)}, u32[]{:S(2)}, u32[]{:S(2)}) async-start(bf16[16,64,512]{2,1,0:T(8,128)(2,1)} %reduce_sum.60), calls=%async_computation.6 | async-start | bytes 2097152 | tf_op jit(solution)/shard_map/all_to_all | solution.py:70
  167.4 5.5 %copy-start.2 = (bf16[1,2048,768]{1,2,0:T(8,128)(2,1)S(1)}, bf16[1,2048,768]{1,2,0:T(8,128)(2,1)}, u32[]{:S(2)}) copy-start(bf16[1,2048,768]{1,2,0:T(8,128)(2,1)} %fusion.10) | copy-start | bytes 9437188
  175.6 5.5 %copy-start.8 = (bf16[128,512]{1,0:T(8,128)(2,1)S(1)}, bf16[128,512]{1,0:T(8,128)(2,1)}, u32[]{:S(2)}) copy-start(bf16[128,512]{1,0:T(8,128)(2,1)} %param.21) | copy-start | bytes 393220
  175.6 6.3 %copy-start.9 = (bf16[128,512]{1,0:T(8,128)(2,1)S(1)}, bf16[128,512]{1,0:T(8,128)(2,1)}, u32[]{:S(2)}) copy-start(bf16[128,512]{1,0:T(8,128)(2,1)} %param.22) | copy-start | bytes 393220
  175.6 11.7 %copy-start.1 = (bf16[1,2048,768]{2,1,0:T(8,128)(2,1)S(1)}, bf16[1,2048,768]{2,1,0:T(8,128)(2,1)}, u32[]{:S(2)}) copy-start(bf16[1,2048,768]{2,1,0:T(8,128)(2,1)} %param.17) | copy-start | bytes 9437188
where the time goes:
time: 188 us; the launch traced here: 187 us
  waiting for transfers between devices  50.1 us (27%)
  blocking collectives  44.5 us (24%)
  matrix products  36.5 us (19%)
  local copies, waits for them, and re-layouts  26.1 us (14%)
  starting transfers between devices  21.8 us (12%)
  other arithmetic  7.33 us (4%)
    all_to_all x1, waiting for transfers between devices, sum_at_owner(): pieces = lax.all_to_all(cut_along(x, dim, devices), axis, 0, 0, tiled=True)  25.7 us
    all_to_all x1, blocking collectives, expert_pass(): lax.all_to_all(outgoing, SP, split_axis=0, concat_axis=1, tiled=True)  19.9 us
    all_to_all x1, waiting for transfers between devices, sent_to_all(): lax.all_to_all(jnp.broadcast_to(x[None], (devices, *x.shape)), axis, 0, 0...  19.3 us
    dot_general x5, matrix products, contract_first(): lax.dot_general(left, right, (((0,), (0,)), ((), ())), preferred_element_...  15.7 us
    all_gather x1, blocking collectives, per_device(): resid_full = lax.all_gather(resid_grad, 'tp', axis=1, tiled=True)  13.4 us
    dot_general x3, matrix products, contract_last(): lax.dot_general(left, right, (((1,), (1,)), ((), ())), preferred_element_...  10.6 us
    unnamed x44, local copies, waits for them, and re-layouts  9.99 us
    all_to_all x1, blocking collectives, sum_at_owner(): pieces = lax.all_to_all(cut_along(x, dim, devices), axis, 0, 0, tiled=True)  6.85 us
  transfers between devices with their start and end apart: 6, of which 4 were waited for; matrix products, arithmetic and copies ran while one was open for 18% of the time, Pallas kernels for 0%

commit v1 on v0

v1 whole, which is shorter than its diff:
```python
import functools
import math

import jax
import jax.numpy as jnp
from jax import lax
from jax.experimental import pallas as pl
from jax.experimental.pallas import tpu as pltpu
from jax.sharding import PartitionSpec as P

MESH = pl.DeviceIdType.MESH
BF = jnp.bfloat16
F32 = jnp.float32

Z, Y, C = 4, 4, 2
SP = Z * Y * C
TP = 4
TOK = 128
CAP = 16
SLOTS = SP * CAP
CH = 512
HID = 768
ROWS = 64
GROUP = Y * C
CHUNK = GROUP * CAP
ORDER = (0, 1, 3, 2)


def mm(a, b, dims):
    return lax.dot_general(a, b, ((dims[:1], dims[1:]), ((), ())), preferred_element_type=F32)


def at(block, size):
    return pl.ds(pl.multiple_of(block * size, size), size)


def layer_kernel(
    ids_hbm, w_hbm, og_hbm, inp_hbm, gw_hbm, uw_hbm, dw_hbm,
    gate_hbm, ing_hbm, val_hbm, conv_hbm, taps_hbm, pw_hbm,
    resid_out, ogg_out, igg_out, vg_out, proj_out, routed_out, hid_out, dgu_out,
    ids_v, w_v, og_v, inp_v, gu_v, dw_v, gate_v, ing_v, val_v, conv_v, taps_v, pw_v,
    ogopp_v, disp_v, wslot_v, out0_v, out2_v, r_v, s_v, a_v, hid_v, dgu_v,
    p_v, rp_v, b0_v, ret0_v, ret2_v, m2_v, r2_v, rf_v, resid_v, cg_v, before_v, after_v,
    ogg_v, igg_v, vg_v, z_v, pp_v, pair_v, q_v, rq_v, proj_v,
    ld_sem, st_sem, ogopp_sem, disp_sem, recv0_sem, recv2_sem, x_send, x_recv,
    pn_send, pn_recv, ret_send, ret_recv, m2_sem, rf_send, rf_recv, halo_sem, pair_sem,
    rq_send, rq_recv,
):
    sp = lax.axis_index("sp")
    x = lax.axis_index("tp")
    z = sp // GROUP
    inner = lax.rem(sp, GROUP)
    core = lax.rem(sp, C)
    chip = sp // C
    xp, xm, xo = lax.rem(x + 1, TP), lax.rem(x + 3, TP), lax.rem(x + 2, TP)

    def load(i, src, dst):
        copy = pltpu.make_async_copy(src, dst, ld_sem.at[i])
        copy.start()
        return copy

    loads = [
        load(0, ids_hbm, ids_v),
        load(1, w_hbm, w_v),
        load(2, og_hbm, og_v),
        load(3, inp_hbm, inp_v),
        load(4, gw_hbm, gu_v.at[:, pl.ds(0, HID)]),
        load(5, uw_hbm, gu_v.at[:, pl.ds(HID, HID)]),
        load(6, dw_hbm, dw_v),
        load(7, gate_hbm, gate_v),
        load(8, conv_hbm, conv_v),
        load(9, pw_hbm, pw_v),
        load(10, ing_hbm, ing_v),
        load(11, val_hbm, val_v),
        load(12, taps_hbm, taps_v),
    ]

    barrier = pltpu.get_barrier_semaphore()

    def greet(i, carry):
        other = lax.rem(sp + 1 + i, SP)
        pl.semaphore_signal(barrier, inc=1, device_id=(other, x), device_id_type=MESH)
        return carry

    lax.fori_loop(0, SP - 1, greet, 0)
    for t in (xp, xm, xo):
        pl.semaphore_signal(barrier, inc=1, device_id=(sp, t), device_id_type=MESH)

    loads[0].wait()
    loads[1].wait()
    loads[2].wait()
    ids = ids_v[...]
    wts = w_v[...]
    e_iota = lax.broadcasted_iota(jnp.int32, (SP, TOK), 0)
    first = e_iota == ids[0:1, :]
    second = e_iota == ids[1:2, :]
    named = jnp.where(first | second, 1.0, 0.0)
    w_et = jnp.where(first, wts[0:1, :], 0.0) + jnp.where(second, wts[1:2, :], 0.0)
    earlier = lax.broadcasted_iota(jnp.int32, (TOK, TOK), 0) < lax.broadcasted_iota(
        jnp.int32, (TOK, TOK), 1
    )
    prefix = mm(named.astype(BF), jnp.where(earlier, 1.0, 0.0).astype(BF), (1, 0))
    rank = jnp.where(named > 0.5, prefix, -1.0)
    r_iota = lax.broadcasted_iota(jnp.int32, (SP, CAP, TOK), 1).astype(F32)
    hit = jnp.broadcast_to(rank[:, None, :], (SP, CAP, TOK)) == r_iota
    disp = jnp.where(hit, 1.0, 0.0)
    wslot = jnp.sum(disp * w_et[:, None, :], axis=2, keepdims=True)
    disp_v[...] = disp.reshape(SLOTS, TOK).astype(BF)
    wslot_v[...] = jnp.broadcast_to(wslot, (SP, CAP, TOK)).reshape(SLOTS, TOK)

    def dispatch(tok_ref, out_ref):
        rows = mm(disp_v[...], tok_ref[...], (1, 0))
        out_ref[...] = (rows * jnp.tile(wslot_v[...], (1, CH // TOK))).astype(BF)

    dispatch(og_v, out0_v)
    pl.semaphore_wait(barrier, SP - 1 + TP - 1)

    ogopp = pltpu.make_async_remote_copy(
        og_v, ogopp_v, ogopp_sem.at[0], ogopp_sem.at[1], device_id=(sp, xo), device_id_type=MESH
    )
    ogopp.start()

    def scatter(out_ref, block, which, recv_sem):
        r_v[block, at(sp, CAP), :] = out_ref[at(sp, CAP), :]
        for dz in ORDER:
            home = lax.rem(z - dz + Z, Z) * GROUP

            def send(i, carry):
                there = home + (lax.rem(inner + 1 + i, GROUP) if dz == 0 else lax.rem(inner + i, GROUP))
                pltpu.make_async_remote_copy(
                    out_ref.at[at(there, CAP), :],
                    r_v.at[block, at(sp, CAP), :],
                    disp_sem.at[which],
                    recv_sem.at[dz],
                    device_id=(there, x),
                    device_id_type=MESH,
                ).start()
                return carry

            lax.fori_loop(0, GROUP - 1 if dz == 0 else GROUP, send, 0)

    def await_bytes(ref, sem):
        pltpu.make_async_copy(ref, ref, sem).wait()

    def chunk_rows(dz):
        return at(lax.rem(z + dz, Z), CHUNK)

    scatter(out0_v, 0, 0, recv0_sem)

    x_copies = []

    def await_group(block, dz, recv_sem):
        count = CHUNK - CAP if dz == 0 else CHUNK
        await_bytes(r_v.at[block, pl.ds(0, count), :], recv_sem.at[dz])

    def forward(k):
        dz = ORDER[k]
        await_group(0, dz, recv0_sem)
        for way, (there, landing) in enumerate(((xp, 3), (xm, 1))):
            copy = pltpu.make_async_remote_copy(
                r_v.at[0, chunk_rows(dz), :],
                r_v.at[landing, chunk_rows(dz), :],
                x_send.at[way, k],
                x_recv.at[way, k],
                device_id=(sp, there),
                device_id_type=MESH,
            )
            copy.start()
            x_copies.append(copy)

    TILE = 256

    def hidden_tile(n):
        cols = slice(n * TILE, (n + 1) * TILE)
        ups = slice(HID + n * TILE, HID + (n + 1) * TILE)

        def rows_of(m, carry):
            rows = at(m, 256)
            pre_gate = mm(inp_v[rows, :], gu_v[:, cols], (1, 0))
            pre_up = mm(inp_v[rows, :], gu_v[:, ups], (1, 0))
            sig = 1.0 / (1.0 + jnp.exp(-pre_gate))
            act = pre_gate * sig
            s_v[rows, cols] = act
            a_v[rows, cols] = pre_up * sig * (1.0 + pre_gate * (1.0 - sig))
            hid_v[rows, cols] = (act * pre_up).astype(BF)
            return carry

        lax.fori_loop(0, SLOTS // 256, rows_of, 0)

    loads[3].wait()
    loads[4].wait()
    loads[5].wait()
    hidden_tile(0)
    ogopp.wait_recv()
    dispatch(ogopp_v, out2_v)
    scatter(out2_v, 2, 1, recv2_sem)
    forward(0)
    forward(1)
    hidden_tile(1)
    forward(2)
    forward(3)
    hidden_tile(2)
    stores = []

    def store(i, src, dst):
        copy = pltpu.make_async_copy(src, dst, st_sem.at[i])
        copy.start()
        stores.append(copy)

    store(0, hid_v, hid_out)
    loads[6].wait()

    p_copies = {}

    def give_back(src_ref, dst_ref, which, dz):
        home = lax.rem(z + dz, Z) * GROUP
        if dz == 0:
            dst_ref[at(sp, CAP), :] = src_ref[at(sp, CAP), :]

        def send(i, carry):
            there = home + (lax.rem(inner + 1 + i, GROUP) if dz == 0 else lax.rem(inner + i, GROUP))
            pltpu.make_async_remote_copy(
                src_ref.at[at(there, CAP), :],
                dst_ref.at[at(sp, CAP), :],
                ret_send.at[which],
                ret_recv.at[which],
                device_id=(there, x),
                device_id_type=MESH,
            ).start()
            return carry

        lax.fori_loop(0, GROUP - 1 if dz == 0 else GROUP, send, 0)

    def finish_own(k):
        dz = ORDER[k]
        rows = chunk_rows(dz)
        for way in range(2):
            p_copies[way, k].wait_recv()
        total = p_v[0, rows, :].astype(F32) + rp_v[0, rows, :].astype(F32) + rp_v[1, rows, :].astype(F32)
        b0_v[rows, :] = total.astype(BF)
        give_back(b0_v, ret0_v, 0, dz)

    for k, dz in enumerate(ORDER):
        rows = chunk_rows(dz)
        await_group(2, dz, recv2_sem)
        x_copies[2 * k].wait_recv()
        x_copies[2 * k + 1].wait_recv()
        d_hidden = None
        for j in range(TP):
            term = mm(r_v[j, rows, :], dw_v[:, at(lax.rem(x + j, TP), CH)], (1, 1))
            d_hidden = term if d_hidden is None else d_hidden + term
        dgu_v[rows, 0:HID] = (d_hidden * a_v[rows, :]).astype(BF)
        dgu_v[rows, HID : 2 * HID] = (d_hidden * s_v[rows, :]).astype(BF)
        for j in (1, 3, 2, 0):
            part = mm(dgu_v[rows, :], gu_v[at(lax.rem(x + j, TP), CH), :], (1, 1))
            p_v[j, rows, :] = part.astype(BF)
            if j in (1, 3):
                way = 0 if j == 1 else 1
                copy = pltpu.make_async_remote_copy(
                    p_v.at[j, rows, :],
                    rp_v.at[way, rows, :],
                    pn_send.at[way, k],
                    pn_recv.at[way, k],
                    device_id=(sp, xp if j == 1 else xm),
                    device_id_type=MESH,
                )
                copy.start()
                p_copies[way, k] = copy
            if j == 2:
                give_back(p_v.at[2], ret2_v, 1, dz)
        if k > 0:
            finish_own(k - 1)
    finish_own(Z - 1)
    for j in range(TP):
        store(1 + j, r_v.at[j], routed_out.at[lax.rem(x + j, TP)])
    store(5, dgu_v, dgu_out)

    loads[7].wait()
    loads[8].wait()
    gate_vals = gate_v[...].astype(F32)
    conv_vals = conv_v[...].astype(F32)
    z_v[...] = (gate_vals * conv_vals).astype(BF)

    def await_returned(ref, which):
        await_bytes(ref.at[pl.ds(0, SLOTS - CAP), :], ret_recv.at[which])

    await_returned(ret2_v, 1)
    m2_v[...] = mm(disp_v[...], ret2_v[...], (0, 0)).astype(BF)
    m2 = pltpu.make_async_remote_copy(
        m2_v, r2_v, m2_sem.at[0], m2_sem.at[1], device_id=(sp, xo), device_id_type=MESH
    )
    m2.start()
    await_returned(ret0_v, 0)
    own = og_v[...].astype(F32) + mm(disp_v[...], ret0_v[...], (0, 0))
    m2.wait_recv()
    rf_v[0] = (own + r2_v[...].astype(F32)).astype(BF)
    rf_copies = []
    for i, (there, landing) in enumerate(((xp, 3), (xm, 1), (xo, 2))):
        copy = pltpu.make_async_remote_copy(
            rf_v.at[0],
            rf_v.at[landing],
            rf_send.at[i],
            rf_recv.at[i],
            device_id=(sp, there),
            device_id_type=MESH,
        )
        copy.start()
        rf_copies.append(copy)
    store(6, rf_v.at[0], resid_out)
    loads[9].wait()

    def proj_part(j):
        part = mm(rf_v[j], z_v[...], (0, 0)).astype(BF)
        pp_v[at(lax.rem(x + j, TP), Y)] = part.reshape(Y, C, ROWS, CH)

    mix = mm(rf_v[0], pw_v[at(x, CH), :], (1, 0))
    proj_part(0)
    for j, i in ((3, 0), (1, 1), (2, 2)):
        rf_copies[i].wait_recv()
        mix = mix + mm(rf_v[j], pw_v[at(lax.rem(x + j, TP), CH), :], (1, 0))
        proj_part(j)
    partner = sp + 1 - 2 * core
    pair = pltpu.make_async_remote_copy(
        pp_v.at[:, 1 - core],
        pair_v,
        pair_sem.at[0],
        pair_sem.at[1],
        device_id=(partner, x),
        device_id_type=MESH,
    )
    pair.start()
    ogg_v[...] = (mix * conv_vals).astype(BF)
    cg_v[...] = (mix * gate_vals).astype(BF)
    down = pltpu.make_async_remote_copy(
        cg_v.at[pl.ds(0, 16), :], after_v, halo_sem.at[0], halo_sem.at[1],
        device_id=(lax.rem(sp + SP - 1, SP), x), device_id_type=MESH,
    )
    up = pltpu.make_async_remote_copy(
        cg_v.at[pl.ds(TOK - 16, 16), :], before_v, halo_sem.at[2], halo_sem.at[3],
        device_id=(lax.rem(sp + 1, SP), x), device_id_type=MESH,
    )
    down.start()
    up.start()
    store(7, ogg_v, ogg_out)
    pair.wait_recv()

    def add_pair(i, carry):
        total = pp_v[i, core].astype(F32) + pair_v[i].astype(F32)
        q_v[i] = total.astype(BF)
        return carry

    lax.fori_loop(0, Z * Y, add_pair, 0)

    def reduce_send(i, carry):
        there = lax.rem(chip + 1 + i, Z * Y)
        pltpu.make_async_remote_copy(
            q_v.at[there],
            rq_v.at[chip],
            rq_send.at[0],
            rq_recv.at[0],
            device_id=(there * C + core, x),
            device_id_type=MESH,
        ).start()
        return carry

    lax.fori_loop(0, Z * Y - 1, reduce_send, 0)
    rq_v[chip] = q_v[chip]

    loads[10].wait()
    loads[11].wait()
    loads[12].wait()
    down.wait_recv()
    up.wait_recv()
    cg = cg_v[...].astype(F32)
    taps = taps_v[...].astype(F32)
    row = lax.broadcasted_iota(jnp.int32, (TOK, CH), 0)
    has_before = jnp.where(sp > 0, 1.0, 0.0)
    has_after = jnp.where(sp < SP - 1, 1.0, 0.0)
    before = before_v[...].astype(F32)[15:16, :] * has_before
    after = after_v[...].astype(F32)[0:1, :] * has_after
    nxt = jnp.where(row == TOK - 1, jnp.broadcast_to(after, (TOK, CH)), pltpu.roll(cg, TOK - 1, 0))
    prv = jnp.where(row == 0, jnp.broadcast_to(before, (TOK, CH)), pltpu.roll(cg, 1, 0))
    value_grad = nxt * taps[0:1, :] + cg * taps[1:2, :] + prv * taps[2:3, :]
    igg_v[...] = (value_grad * val_v[...].astype(F32)).astype(BF)
    vg_v[...] = (value_grad * ing_v[...].astype(F32)).astype(BF)
    store(8, igg_v, igg_out)
    store(9, vg_v, vg_out)

    await_bytes(rq_v.at[pl.ds(0, Z * Y - 1)], rq_recv.at[0])
    total = rq_v[0].astype(F32)
    for i in range(1, Z * Y):
        total = total + rq_v[i].astype(F32)
    proj_v[...] = total * (1.0 / math.sqrt(TOK * SP))
    store(10, proj_v, proj_out)

    ogopp.wait_send()
    for which, ref in ((0, out0_v), (1, out2_v)):
        await_bytes(ref.at[pl.ds(0, SLOTS - CAP), :], disp_sem.at[which])
        await_bytes(ref.at[pl.ds(0, SLOTS - CAP), :], ret_send.at[which])
    for copy in x_copies:
        copy.wait_send()
    for copy in p_copies.values():
        copy.wait_send()
    m2.wait_send()
    for copy in rf_copies:
        copy.wait_send()
    down.wait_send()
    up.wait_send()
    pair.wait_send()
    await_bytes(rq_v.at[pl.ds(0, Z * Y - 1)], rq_send.at[0])
    for copy in stores:
        copy.wait()


def grads_kernel(
    inp_ref, dgu_ref, hid_ref, routed_ref, resid_ref, ogg_ref, igg_ref, vg_ref, proj_ref,
    gate_out, up_out, down_out, resid_out, ogg_out, igg_out, vg_out, proj_out,
):
    scale = 1.0 / math.sqrt(SLOTS)
    both = mm(inp_ref[0], dgu_ref[...], (0, 0)) * scale
    gate_out[0] = both[:, :HID].astype(BF)
    up_out[0] = both[:, HID:].astype(BF)
    down_out[0] = (mm(hid_ref[...], routed_ref[0], (0, 0)) * scale).astype(BF)
    resid_out[...] = resid_ref[...]
    ogg_out[...] = ogg_ref[...]
    igg_out[...] = igg_ref[...]
    vg_out[...] = vg_ref[...]
    proj_out[...] = proj_ref[...]


def per_device(
    out_grad, route_ids, route_weight, expert_inputs, gate_weight, up_weight, down_weight,
    out_gate, in_gate, values, conv_out, conv_taps, proj_weight,
):
    sds = jax.ShapeDtypeStruct
    hbm = pl.BlockSpec(memory_space=pl.ANY)
    vm = pltpu.VMEM
    dma = pltpu.SemaphoreType.DMA
    act = (TOK, CH)
    outs = pl.pallas_call(
        layer_kernel,
        in_specs=[hbm] * 13,
        out_specs=[hbm] * 8,
        out_shape=[
            sds(act, BF), sds(act, BF), sds(act, BF), sds(act, BF), sds((ROWS, CH), F32),
            sds((TP, SLOTS, CH), BF), sds((SLOTS, HID), BF), sds((SLOTS, 2 * HID), BF),
        ],
        scratch_shapes=[
            vm((2, TOK), jnp.int32), vm((2, TOK), F32), vm(act, BF), vm((SLOTS, TP * CH), BF),
            vm((TP * CH, 2 * HID), BF), vm((HID, TP * CH), BF), vm(act, BF), vm(act, BF), vm(act, BF),
            vm(act, BF), vm((3, CH), BF), vm((TP * CH, CH), BF),
            vm(act, BF), vm((SLOTS, TOK), BF), vm((SLOTS, TOK), F32), vm((SLOTS, CH), BF),
            vm((SLOTS, CH), BF), vm((TP, SLOTS, CH), BF), vm((SLOTS, HID), F32), vm((SLOTS, HID), F32),
            vm((SLOTS, HID), BF), vm((SLOTS, 2 * HID), BF),
            vm((TP, SLOTS, CH), BF), vm((2, SLOTS, CH), BF), vm((SLOTS, CH), BF), vm((SLOTS, CH), BF),
            vm((SLOTS, CH), BF), vm(act, BF), vm(act, BF), vm((TP,) + act, BF), vm(act, BF), vm(act, BF),
            vm((16, CH), BF), vm((16, CH), BF),
            vm(act, BF), vm(act, BF), vm(act, BF), vm(act, BF), vm((Z * Y, C, ROWS, CH), BF),
            vm((Z * Y, ROWS, CH), BF), vm((Z * Y, ROWS, CH), BF), vm((Z * Y, ROWS, CH), BF),
            vm((ROWS, CH), F32),
            dma((13,)), dma((11,)), dma((2,)), dma((2,)), dma((Z,)), dma((Z,)), dma((2, Z)), dma((2, Z)),
            dma((2, Z)), dma((2, Z)), dma((2,)), dma((2,)), dma((2,)), dma((3,)), dma((3,)), dma((4,)),
            dma((2,)), dma((1,)), dma((1,)),
        ],
        compiler_params=pltpu.CompilerParams(
            collective_id=0, has_side_effects=True, vmem_limit_bytes=62 * 1024 * 1024
        ),
    )(
        route_ids.T, route_weight.T, out_grad, expert_inputs[0], gate_weight[0], up_weight[0],
        down_weight[0], out_gate, in_gate, values, conv_out, conv_taps, proj_weight,
    )
    resid, ogg, igg, vg, proj, routed, hid, dgu = outs
    steps = TP

    def whole(shape):
        return pl.BlockSpec(shape, lambda i: (0,) * len(shape))

    def strip(rows, cols=CH):
        return pl.BlockSpec((rows // steps, cols), lambda i: (i, 0))

    gate_grad, up_grad, down_grad, resid, ogg, igg, vg, proj = pl.pallas_call(
        grads_kernel,
        grid=(steps,),
        in_specs=[
            pl.BlockSpec((1, SLOTS, CH), lambda i: (0, 0, i)),
            whole((SLOTS, 2 * HID)),
            whole((SLOTS, HID)),
            pl.BlockSpec((1, SLOTS, CH), lambda i: (i, 0, 0)),
            strip(TOK), strip(TOK), strip(TOK), strip(TOK), strip(ROWS),
        ],
        out_specs=[
            pl.BlockSpec((1, CH, HID), lambda i: (0, i, 0)),
            pl.BlockSpec((1, CH, HID), lambda i: (0, i, 0)),
            pl.BlockSpec((1, HID, CH), lambda i: (0, 0, i)),
            strip(TOK), strip(TOK), strip(TOK), strip(TOK), strip(ROWS),
        ],
        out_shape=[
            sds((1, TP * CH, HID), BF), sds((1, TP * CH, HID), BF), sds((1, HID, TP * CH), BF),
            sds(act, BF), sds(act, BF), sds(act, BF), sds(act, BF), sds((ROWS, CH), F32),
        ],
        compiler_params=pltpu.CompilerParams(
            dimension_semantics=("arbitrary",), vmem_limit_bytes=48 * 1024 * 1024
        ),
    )(expert_inputs, dgu, hid, routed, resid, ogg, igg, vg, proj)
    return resid, ogg, igg, vg, proj, gate_grad, up_grad, down_grad


def solution(mesh):
    return jax.shard_map(
        per_device,
        mesh=mesh,
        in_specs=(
            P("sp", "tp"), P("sp", None), P("sp", None), P("sp", None, None), P("sp", None, "tp"),
            P("sp", None, "tp"), P("sp", "tp", None), P("sp", "tp"), P("sp", "tp"), P("sp", "tp"),
            P("sp", "tp"), P(None, "tp"), P(None, "tp"),
        ),
        out_specs=(
            P("sp", "tp"), P("sp", "tp"), P("sp", "tp"), P("sp", "tp"), P("sp", "tp"),
            P("sp", None, "tp"), P("sp", None, "tp"), P("sp", "tp", None),
        ),
        check_vma=False,
    )
```

time: 188 us -> 99.7 us (0.53)
  Pallas kernels: 0 us -> 88.7 us
  waiting for transfers between devices: 50.1 us -> 0 us
  blocking collectives: 44.5 us -> 0 us
  matrix products: 36.5 us -> 0 us
  starting transfers between devices: 21.8 us -> 0 us
  local copies, waits for them, and re-layouts: 26.1 us -> 8.64 us
  other arithmetic: 7.33 us -> 0 us
    pallas_call x0 -> x2, Pallas kernels: none -> 88.7 us  [the longest x1 80.7 us: per_device(): pl.pallas_call(layer_kernel, in_specs=[hbm] * 13, out_specs=[hbm] * 8, ou...]
    all_to_all x4 -> x0, waiting for transfers between devices: 50.1 us -> none  [the longest x1 25.7 us: sum_at_owner(): pieces = lax.all_to_all(cut_along(x, dim, devices), axis, 0, 0, tiled=True)]
    dot_general x12 -> x0, matrix products: 36.5 us -> none  [the longest x5 15.7 us: contract_first(): lax.dot_general(left, right, (((0,), (0,)), ((), ())), preferred_element_...]
    all_to_all x3 -> x0, blocking collectives: 31.1 us -> none  [the longest x1 19.9 us: expert_pass(): lax.all_to_all(outgoing, SP, split_axis=0, concat_axis=1, tiled=True)]
    all_to_all x4 -> x0, starting transfers between devices: 19.2 us -> none  [the longest x1 6.5 us: sum_by_axis(): lax.all_to_all(own.astype(jnp.bfloat16), far, 0, 0, tiled=True)]
    all_gather x1 -> x0, blocking collectives: 13.4 us -> none  [per_device(): resid_full = lax.all_gather(resid_grad, 'tp', axis=1, tiled=True)]
    reshape x2 -> x0, local copies, waits for them, and re-layouts: 5.04 us -> none  [cut_along(): x.reshape(*lengths[:dim], devices, lengths[dim] // devices, *lengths[dim...]
    broadcast_in_dim x2 -> x0, local copies, waits for them, and re-layouts: 4.57 us -> none  [sent_to_all(): jnp.broadcast_to(x[None], (devices, *x.shape))]
  transfers between devices with their start and end apart: 6 -> 0, of which waited for: 4 -> 0; matrix products, arithmetic and copies ran while one was open for 18% -> 0% of each run, Pallas kernels for 0% -> 0%
where the time goes in v1:
time: 99.7 us; the launch traced here: 98 us
  Pallas kernels  88.7 us (89%)
  local copies, waits for them, and re-layouts  8.64 us (9%)
    pallas_call x1, Pallas kernels, per_device(): pl.pallas_call(layer_kernel, in_specs=[hbm] * 13, out_specs=[hbm] * 8, ou...  80.7 us
    unnamed x16, local copies, waits for them, and re-layouts  8.64 us
    pallas_call x1, Pallas kernels, per_device(): pl.pallas_call(grads_kernel, grid=(steps,), in_specs=[pl.BlockSpec((1, SL...  8.05 us

profile of v1, /device:TPU:0, one launch (start us, length us, event | category | flops | bytes accessed | tf_op | source)
XLA Modules:
  0.0 98.0 jit_solution(3646329979510568272)
XLA Ops:
  0.6 80.7 %shard_map.188 = (bf16[128,512]{1,0:T(8,128)(2,1)}, bf16[128,512]{1,0:T(8,128)(2,1)}, bf16[128,512]{1,0:T(8,128)(2,1)}, bf16[128,512]{1,0:T(8,128)(2,1)}, f32[64...) custom-call(s32[2,128]{1,0:T(2,128)} %bitcast.10, ...), custom_call_target="tpu_custom_call" | custom-call | tf_op jit(solution)/shard_map/pallas_call | solution.py:440
  81.3 0.0 copy-start
  81.3 1.6 %copy-done = bf16[1,512,2048]{2,1,0:T(8,128)(2,1)S(1)} copy-done((bf16[1,512,2048]{2,1,0:T(8,128)(2,1)S(1)}, bf16[1,512,2048]{2,1,0:T(8,128)(2,1)}, u32[]{:S(2)}) %copy-start) | copy-done | bytes 2097176
  82.9 0.0 copy-start.1
  82.9 1.4 %copy-done.1 = bf16[512,1536]{1,0:T(8,128)(2,1)S(1)} copy-done((bf16[512,1536]{1,0:T(8,128)(2,1)S(1)}, bf16[512,1536]{1,0:T(8,128)(2,1)}, u32[]{:S(2)}) %copy-start.1) | copy-done | bytes 1572888
  84.3 0.0 copy-start.2
  84.3 1.1 %copy-done.2 = bf16[512,768]{1,0:T(8,128)(2,1)S(1)} copy-done((bf16[512,768]{1,0:T(8,128)(2,1)S(1)}, bf16[512,768]{1,0:T(8,128)(2,1)}, u32[]{:S(2)}) %copy-start.2) | copy-done | bytes 786456
  85.5 0.0 copy-start.3
  85.5 0.9 copy-done.3
  86.4 0.0 copy-start.4
  86.4 0.9 copy-done.4
  87.3 0.0 copy-start.5
  87.3 0.9 copy-done.5
  88.2 0.0 copy-start.6
  88.2 0.9 copy-done.6
  89.1 0.0 copy-start.7
  89.1 0.9 copy-done.7
  90.0 8.1 %shard_map.189 = (bf16[1,2048,768]{2,1,0:T(8,128)(2,1)}, bf16[1,2048,768]{2,1,0:T(8,128)(2,1)}, bf16[1,768,2048]{2,1,0:T(8,128)(2,1)}, bf16[128,512]{1,0:T(8,128...) custom-call(bf16[1,512,2048]{2,1,0:T(8,128)(2,1)S(1)} %copy-done, ...), custom_call_target="tpu_custom_call" | custom-call | tf_op jit(solution)/shard_map/pallas_call | solution.py:481
Async XLA Ops:
  81.3 1.6 %copy-start = (bf16[1,512,2048]{2,1,0:T(8,128)(2,1)S(1)}, bf16[1,512,2048]{2,1,0:T(8,128)(2,1)}, u32[]{:S(2)}) copy-start(bf16[1,512,2048]{2,1,0:T(8,128)(2,1)} %inp_ref.1) | copy-start | bytes 6291460
  82.9 1.4 %copy-start.1 = (bf16[512,1536]{1,0:T(8,128)(2,1)S(1)}, bf16[512,1536]{1,0:T(8,128)(2,1)}, u32[]{:S(2)}) copy-start(bf16[512,1536]{1,0:T(8,128)(2,1)} %get-tuple-element.24.dgu_ref) | copy-start | bytes 4718596
  84.3 1.1 %copy-start.2 = (bf16[512,768]{1,0:T(8,128)(2,1)S(1)}, bf16[512,768]{1,0:T(8,128)(2,1)}, u32[]{:S(2)}) copy-start(bf16[512,768]{1,0:T(8,128)(2,1)} %get-tuple-element.25.hid_ref) | copy-start | bytes 2359300
  85.5 0.9 copy-start.3
  86.4 0.9 copy-start.4
  87.3 0.9 copy-start.5
  88.2 0.9 copy-start.6
  89.1 0.9 copy-start.7

commit v2 on v1

v2 whole, which is shorter than its diff:
```python
import functools
import math

import jax
import jax.numpy as jnp
from jax import lax
from jax.experimental import pallas as pl
from jax.experimental.pallas import tpu as pltpu
from jax.sharding import PartitionSpec as P

MESH = pl.DeviceIdType.MESH
BF = jnp.bfloat16
F32 = jnp.float32

Z, Y, C = 4, 4, 2
SP = Z * Y * C
TP = 4
TOK = 128
CAP = 16
SLOTS = SP * CAP
CH = 512
HID = 768
ROWS = 64
GROUP = Y * C
CHUNK = GROUP * CAP
ORDER = (0, 2, 1, 3)
FAR_FIRST = (2, 1, 3, 0)


def mm(a, b, dims):
    return lax.dot_general(a, b, ((dims[:1], dims[1:]), ((), ())), preferred_element_type=F32)


def at(block, size):
    return pl.ds(pl.multiple_of(block * size, size), size)


def layer_kernel(
    ids_hbm, w_hbm, og_hbm, inp_hbm, gw_hbm, uw_hbm, dw_hbm,
    gate_hbm, ing_hbm, val_hbm, conv_hbm, taps_hbm, pw_hbm,
    resid_v, ogg_v, igg_v, vg_v, proj_v, gate_grad_v, up_grad_v, down_grad_v,
    ids_v, w_v, og_v, inp_v, gu_v, dw_v, gate_v, ing_v, val_v, conv_v, taps_v, pw_v,
    ogopp_v, disp_v, wslot_v, out0_v, out2_v, r_v, s_v, a_v, hid_v, dgu_v,
    p_v, rp_v, b0_v, ret0_v, ret2_v, m2_v, r2_v, m0_v, rm0_v, rf_v, cg_v, before_v, after_v,
    zall_v, rft_v, rt_v,
    ld_sem, ogopp_sem, disp_sem, recv0_sem, recv2_sem, x_send, x_recv,
    pn_send, pn_recv, ret_send, ret_recv, m2_sem, m0_sem, rf_send, rf_recv, halo_sem, za_send, za_recv,
    zd_sem, rt_send, rt_recv,
):
    sp = lax.axis_index("sp")
    x = lax.axis_index("tp")
    z = sp // GROUP
    inner = lax.rem(sp, GROUP)
    core = lax.rem(sp, C)
    chip = sp // C
    y = lax.rem(chip, Y)
    xp, xm, xo = lax.rem(x + 1, TP), lax.rem(x + 3, TP), lax.rem(x + 2, TP)

    def load(i, src, dst):
        copy = pltpu.make_async_copy(src, dst, ld_sem.at[i])
        copy.start()
        return copy

    loads = [
        load(0, ids_hbm, ids_v),
        load(1, w_hbm, w_v),
        load(2, og_hbm, og_v),
        load(3, inp_hbm, inp_v),
        load(4, gw_hbm, gu_v.at[:, pl.ds(0, HID)]),
        load(5, uw_hbm, gu_v.at[:, pl.ds(HID, HID)]),
        load(6, dw_hbm, dw_v),
        load(7, gate_hbm, gate_v),
        load(8, conv_hbm, conv_v),
        load(9, pw_hbm, pw_v),
        load(10, ing_hbm, ing_v),
        load(11, val_hbm, val_v),
        load(12, taps_hbm, taps_v),
    ]

    barrier = pltpu.get_barrier_semaphore()

    def greet(i, carry):
        other = lax.rem(sp + 1 + i, SP)
        pl.semaphore_signal(barrier, inc=1, device_id=(other, x), device_id_type=MESH)
        return carry

    lax.fori_loop(0, SP - 1, greet, 0)
    for t in (xp, xm, xo):
        pl.semaphore_signal(barrier, inc=1, device_id=(sp, t), device_id_type=MESH)

    with jax.named_scope("w_load"):
        loads[0].wait()
        loads[1].wait()
        loads[2].wait()
    ids = ids_v[...]
    wts = w_v[...]
    e_iota = lax.broadcasted_iota(jnp.int32, (SP, TOK), 0)
    first = e_iota == ids[0:1, :]
    second = e_iota == ids[1:2, :]
    named = jnp.where(first | second, 1.0, 0.0)
    w_et = jnp.where(first, wts[0:1, :], 0.0) + jnp.where(second, wts[1:2, :], 0.0)
    earlier = lax.broadcasted_iota(jnp.int32, (TOK, TOK), 0) < lax.broadcasted_iota(
        jnp.int32, (TOK, TOK), 1
    )
    prefix = mm(named.astype(BF), jnp.where(earlier, 1.0, 0.0).astype(BF), (1, 0))
    rank = jnp.where(named > 0.5, prefix, -1.0)
    r_iota = lax.broadcasted_iota(jnp.int32, (SP, CAP, TOK), 1).astype(F32)
    hit = jnp.broadcast_to(rank[:, None, :], (SP, CAP, TOK)) == r_iota
    disp = jnp.where(hit, 1.0, 0.0)
    wslot = jnp.sum(disp * w_et[:, None, :], axis=2, keepdims=True)
    disp_v[...] = disp.reshape(SLOTS, TOK).astype(BF)
    wslot_v[...] = jnp.broadcast_to(wslot, (SP, CAP, TOK)).reshape(SLOTS, TOK)

    def dispatch(tok_ref, out_ref):
        rows = mm(disp_v[...], tok_ref[...], (1, 0))
        out_ref[...] = (rows * jnp.tile(wslot_v[...], (1, CH // TOK))).astype(BF)

    dispatch(og_v, out0_v)
    TILE = 256

    def hidden_tile(n):
        cols = slice(n * TILE, (n + 1) * TILE)
        ups = slice(HID + n * TILE, HID + (n + 1) * TILE)

        def rows_of(m, carry):
            rows = at(m, 256)
            pre_gate = mm(inp_v[rows, :], gu_v[:, cols], (1, 0))
            pre_up = mm(inp_v[rows, :], gu_v[:, ups], (1, 0))
            sig = 1.0 / (1.0 + jnp.exp(-pre_gate))
            act = pre_gate * sig
            s_v[rows, cols] = act
            a_v[rows, cols] = pre_up * sig * (1.0 + pre_gate * (1.0 - sig))
            hid_v[rows, cols] = (act * pre_up).astype(BF)
            return carry

        lax.fori_loop(0, SLOTS // 256, rows_of, 0)

    with jax.named_scope("w_weights"):
        loads[3].wait()
        loads[4].wait()
        loads[5].wait()
    hidden_tile(0)
    with jax.named_scope("w_barrier"):
        pl.semaphore_wait(barrier, SP - 1 + TP - 1)

    ogopp = pltpu.make_async_remote_copy(
        og_v, ogopp_v, ogopp_sem.at[0], ogopp_sem.at[1], device_id=(sp, xo), device_id_type=MESH
    )
    ogopp.start()

    def plane(zz, skip_self):
        peers = []
        for dy in FAR_FIRST:
            for dc in (1, 0):
                if not (skip_self and dy == 0 and dc == 0):
                    peers.append((zz * Y + lax.rem(y + dy, Y)) * C + lax.rem(core + dc, C))
        return peers

    def interleaved(dzs, sign):
        lists = [[(dz, there) for there in plane(lax.rem(z + sign * dz + Z, Z), dz == 0)] for dz in dzs]
        return [entry for i in range(GROUP) for entries in lists for entry in entries[i : i + 1]]

    def scatter(out_ref, block, which, recv_sem, dzs):
        if 0 in dzs:
            r_v[block, at(sp, CAP), :] = out_ref[at(sp, CAP), :]
        for dz, there in interleaved(dzs, -1):
            pltpu.make_async_remote_copy(
                out_ref.at[at(there, CAP), :],
                r_v.at[block, at(sp, CAP), :],
                disp_sem.at[which],
                recv_sem.at[dz],
                device_id=(there, x),
                device_id_type=MESH,
            ).start()

    def await_bytes(ref, sem):
        pltpu.make_async_copy(ref, ref, sem).wait()

    def chunk_rows(dz):
        return at(lax.rem(z + dz, Z), CHUNK)

    scatter(out0_v, 0, 0, recv0_sem, (2, 0))
    scatter(out0_v, 0, 0, recv0_sem, (1, 3))

    x_copies = []

    def await_group(block, dz, recv_sem):
        count = CHUNK - CAP if dz == 0 else CHUNK
        with jax.named_scope(f"w_group{block}_{dz}"):
            await_bytes(r_v.at[block, pl.ds(0, count), :], recv_sem.at[dz])

    def forward(k):
        dz = ORDER[k]
        await_group(0, dz, recv0_sem)
        for way, (there, landing) in enumerate(((xp, 3), (xm, 1))):
            copy = pltpu.make_async_remote_copy(
                r_v.at[0, chunk_rows(dz), :],
                r_v.at[landing, chunk_rows(dz), :],
                x_send.at[way, k],
                x_recv.at[way, k],
                device_id=(sp, there),
                device_id_type=MESH,
            )
            copy.start()
            x_copies.append(copy)

    loads[7].wait()
    loads[8].wait()
    gate_vals = gate_v[...].astype(F32)
    conv_vals = conv_v[...].astype(F32)
    zall_v[core, z, y] = (gate_vals * conv_vals).astype(BF)
    partner = sp + 1 - 2 * core
    zp, zm = lax.rem(z + 1, Z), lax.rem(z + 3, Z)
    yp, ym = lax.rem(y + 1, Y), lax.rem(y + 3, Y)
    west, east = pl.ds(0, CH // 2), pl.ds(CH // 2, CH // 2)
    low, high, full = pl.ds(0, TOK // 2), pl.ds(TOK // 2, TOK // 2), pl.ds(0, TOK)
    every = pl.ds(0, Z)
    z_copies = []

    def spread(phase):
        steps = (
            ((z, y, full, west), (z, y, full, west), (z, y, full, east), (z, y, full, east)),
            ((z, ym, low, west), (z, yp, high, west), (zm, y, low, east), (zp, y, high, east)),
            ((z, every, full, west), (z, every, full, west), (every, y, full, east), (every, y, full, east)),
            ((zm, every, low, west), (zp, every, high, west), (every, ym, low, east), (every, yp, high, east)),
        )[phase]
        along_y, along_z = ((z, yp), (z, ym)), ((zp, y), (zm, y))
        theres = along_y + along_z if phase < 2 else along_z + along_y
        if phase > 0:
            with jax.named_scope(f"w_spread{phase}"):
                for copy in z_copies[-4:]:
                    copy.wait_recv()
        for way, ((bz, by, rows, cols), (tz, ty)) in enumerate(zip(steps, theres)):
            part = zall_v.at[core, bz, by, rows, cols]
            copy = pltpu.make_async_remote_copy(
                part, part, za_send.at[phase, way], za_recv.at[phase, way],
                device_id=((tz * Y + ty) * C + core, x), device_id_type=MESH,
            )
            copy.start()
            z_copies.append(copy)

    spread(0)
    hidden_tile(1)
    forward(0)
    with jax.named_scope("w_ogopp"):
        ogopp.wait_recv()
    dispatch(ogopp_v, out2_v)
    scatter(out2_v, 2, 1, recv2_sem, (2, 0))
    forward(1)
    hidden_tile(2)
    spread(1)
    scatter(out2_v, 2, 1, recv2_sem, (1, 3))
    forward(2)
    forward(3)
    loads[6].wait()

    p_copies = {}

    def give_back(src_ref, dst_ref, which, dzs):
        if 0 in dzs:
            dst_ref[at(sp, CAP), :] = src_ref[at(sp, CAP), :]
        for _, there in interleaved(dzs, 1):
            pltpu.make_async_remote_copy(
                src_ref.at[at(there, CAP), :],
                dst_ref.at[at(sp, CAP), :],
                ret_send.at[which],
                ret_recv.at[which],
                device_id=(there, x),
                device_id_type=MESH,
            ).start()

    def finish_own(k):
        dz = ORDER[k]
        rows = chunk_rows(dz)
        with jax.named_scope(f"w_part{k}"):
            for way in range(2):
                p_copies[way, k].wait_recv()
        total = p_v[0, rows, :].astype(F32) + rp_v[0, rows, :].astype(F32) + rp_v[1, rows, :].astype(F32)
        b0_v[rows, :] = total.astype(BF)
        give_back(b0_v, ret0_v, 0, (dz,))

    def rows_pair(ref, halves):
        return jnp.concatenate([ref[rows, :] for rows in halves], axis=0)

    def put_pair(ref, halves, value):
        for h, rows in enumerate(halves):
            ref[rows, :] = value[h * CHUNK : (h + 1) * CHUNK, :]

    for ks in ((0, 1), (2, 3)):
        halves = [chunk_rows(ORDER[k]) for k in ks]
        for k in ks:
            await_group(2, ORDER[k], recv2_sem)
            with jax.named_scope(f"w_x{k}"):
                x_copies[2 * k].wait_recv()
                x_copies[2 * k + 1].wait_recv()
        d_hidden = None
        for j in range(TP):
            term = mm(rows_pair(r_v.at[j], halves), dw_v[:, at(lax.rem(x + j, TP), CH)], (1, 1))
            d_hidden = term if d_hidden is None else d_hidden + term
        if ks[0] == 0:
            spread(2)
        put_pair(dgu_v.at[:, pl.ds(0, HID)], halves, (d_hidden * rows_pair(a_v, halves)).astype(BF))
        put_pair(dgu_v.at[:, pl.ds(HID, HID)], halves, (d_hidden * rows_pair(s_v, halves)).astype(BF))
        for j in (1, 3, 2, 0):
            part = mm(rows_pair(dgu_v, halves), gu_v[at(lax.rem(x + j, TP), CH), :], (1, 1))
            put_pair(p_v.at[j], halves, part.astype(BF))
            if j in (1, 3):
                way = 0 if j == 1 else 1
                for k, rows in zip(ks, halves):
                    copy = pltpu.make_async_remote_copy(
                        p_v.at[j, rows, :],
                        rp_v.at[way, rows, :],
                        pn_send.at[way, k],
                        pn_recv.at[way, k],
                        device_id=(sp, xp if j == 1 else xm),
                        device_id_type=MESH,
                    )
                    copy.start()
                    p_copies[way, k] = copy
            if j == 2:
                give_back(p_v.at[2], ret2_v, 1, [ORDER[k] for k in ks])
                if ks[0] > 0:
                    spread(3)
        if ks[0] > 0:
            finish_own(0)
            finish_own(1)

    slot_scale = 1.0 / math.sqrt(SLOTS)

    def down_tiles(lower, upper):
        def tile(n, carry):
            rows = at(n, 256)
            turned = hid_v[:, rows].T
            for j in range(TP):
                part = mm(turned, r_v[j], (1, 0)) * slot_scale
                down_grad_v[rows, at(lax.rem(x + j, TP), CH)] = part.astype(BF)
            return carry

        lax.fori_loop(lower, upper, tile, 0)

    def gate_tiles(lower, upper):
        def tile(n, carry):
            rows = at(n, 256)
            turned = inp_v[:, rows].T
            gate_grad_v[rows, :] = (mm(turned, dgu_v[:, 0:HID], (1, 0)) * slot_scale).astype(BF)
            up_grad_v[rows, :] = (mm(turned, dgu_v[:, HID : 2 * HID], (1, 0)) * slot_scale).astype(BF)
            return carry

        lax.fori_loop(lower, upper, tile, 0)

    finish_own(2)
    finish_own(3)
    with jax.named_scope("g_gate"):
        gate_tiles(0, 4)
    with jax.named_scope("w_spread4"):
        for copy in z_copies[-4:]:
            copy.wait_recv()
    to_partner = pltpu.make_async_remote_copy(
        zall_v.at[core], zall_v.at[core], zd_sem.at[0], zd_sem.at[1],
        device_id=(partner, x), device_id_type=MESH,
    )
    to_partner.start()

    def await_returned(ref, which):
        with jax.named_scope(f"w_ret{which}"):
            await_bytes(ref.at[pl.ds(0, SLOTS - CAP), :], ret_recv.at[which])

    def to_opposite(src, dst, sem):
        copy = pltpu.make_async_remote_copy(
            src, dst, sem.at[0], sem.at[1], device_id=(sp, xo), device_id_type=MESH
        )
        copy.start()
        return copy

    await_returned(ret2_v, 1)
    m2_v[...] = mm(disp_v[...], ret2_v[...], (0, 0)).astype(BF)
    m2 = to_opposite(m2_v, r2_v, m2_sem)
    await_returned(ret0_v, 0)
    moe = mm(disp_v[...], ret0_v[...], (0, 0))
    m0_v[...] = moe.astype(BF)
    m0 = to_opposite(m0_v, rm0_v, m0_sem)
    with jax.named_scope("w_m2"):
        m2.wait_recv()
    own = (og_v[...].astype(F32) + moe + r2_v[...].astype(F32)).astype(BF)
    rf_v[0] = own
    rf_copies = []
    for i, (there, landing) in enumerate(((xp, 3), (xm, 1))):
        copy = pltpu.make_async_remote_copy(
            rf_v.at[0],
            rf_v.at[landing],
            rf_send.at[i],
            rf_recv.at[i],
            device_id=(sp, there),
            device_id_type=MESH,
        )
        copy.start()
        rf_copies.append(copy)
    resid_v[...] = own
    loads[9].wait()

    def mix_part(j):
        return mm(rf_v[j], pw_v[at(lax.rem(x + j, TP), CH), :], (1, 0))

    def order_of(cc, zz, yy):
        return (cc * Z + zz) * Y + yy

    mine = order_of(core, z, y)

    def share(j):
        block = lax.rem(x + j, TP)
        rft_v[j] = rf_v[j].T.reshape(GROUP, ROWS, TOK)

        for there in plane(block, False):
            inside = lax.rem(there, GROUP)

            @pl.when(there != sp)
            def _():
                pltpu.make_async_remote_copy(
                    rft_v.at[j, inside],
                    rt_v.at[mine],
                    rt_send.at[0],
                    rt_recv.at[lax.rem(z - block + Z, Z)],
                    device_id=(there, x),
                    device_id_type=MESH,
                ).start()

    share(0)
    mix = mix_part(0)
    with jax.named_scope("g_gate2"):
        gate_tiles(4, 8)
    for j, i in ((3, 0), (1, 1)):
        with jax.named_scope(f"w_rf{j}"):
            rf_copies[i].wait_recv()
        share(j)
        mix = mix + mix_part(j)
    with jax.named_scope("w_rf2"):
        m0.wait_recv()
    rf_v[2] = (ogopp_v[...].astype(F32) + rm0_v[...].astype(F32) + m2_v[...].astype(F32)).astype(BF)
    mix = mix + mix_part(2)
    ogg_v[...] = (mix * conv_vals).astype(BF)
    cg_v[...] = (mix * gate_vals).astype(BF)
    down = pltpu.make_async_remote_copy(
        cg_v.at[pl.ds(0, 16), :], after_v, halo_sem.at[0], halo_sem.at[1],
        device_id=(lax.rem(sp + SP - 1, SP), x), device_id_type=MESH,
    )
    up = pltpu.make_async_remote_copy(
        cg_v.at[pl.ds(TOK - 16, 16), :], before_v, halo_sem.at[2], halo_sem.at[3],
        device_id=(lax.rem(sp + 1, SP), x), device_id_type=MESH,
    )
    down.start()
    up.start()
    share(2)
    rt_v[mine] = rft_v[lax.rem(z - x + TP, TP), inner]
    with jax.named_scope("g_down"):
        down_tiles(0, HID // 256)
    with jax.named_scope("w_zd"):
        to_partner.wait_recv()

    def proj_group(dz):
        count = GROUP - 1 if dz == 0 else GROUP
        with jax.named_scope(f"w_rt{dz}"):
            await_bytes(rt_v.at[pl.ds(0, count)], rt_recv.at[dz])
        zz = lax.rem(z + dz, Z)
        total = None
        for cc in range(C):
            left = jnp.concatenate([rt_v[order_of(cc, zz, yy)] for yy in range(Y)], axis=1)
            term = mm(left, zall_v[cc, zz].reshape(Y * TOK, CH), (1, 0))
            total = term if total is None else total + term
        return total

    proj = proj_group(0) + proj_group(1)

    loads[10].wait()
    loads[11].wait()
    loads[12].wait()
    with jax.named_scope("w_halo"):
        down.wait_recv()
        up.wait_recv()
    cg = cg_v[...].astype(F32)
    taps = taps_v[...].astype(F32)
    row = lax.broadcasted_iota(jnp.int32, (TOK, CH), 0)
    has_before = jnp.where(sp > 0, 1.0, 0.0)
    has_after = jnp.where(sp < SP - 1, 1.0, 0.0)
    before = before_v[...].astype(F32)[15:16, :] * has_before
    after = after_v[...].astype(F32)[0:1, :] * has_after
    nxt = jnp.where(row == TOK - 1, jnp.broadcast_to(after, (TOK, CH)), pltpu.roll(cg, TOK - 1, 0))
    prv = jnp.where(row == 0, jnp.broadcast_to(before, (TOK, CH)), pltpu.roll(cg, 1, 0))
    value_grad = nxt * taps[0:1, :] + cg * taps[1:2, :] + prv * taps[2:3, :]
    igg_v[...] = (value_grad * val_v[...].astype(F32)).astype(BF)
    vg_v[...] = (value_grad * ing_v[...].astype(F32)).astype(BF)

    proj = proj + proj_group(3)
    proj = proj + proj_group(2)
    proj_v[...] = proj * (1.0 / math.sqrt(TOK * SP))

    ogopp.wait_send()
    for which, ref in ((0, out0_v), (1, out2_v)):
        await_bytes(ref.at[pl.ds(0, SLOTS - CAP), :], disp_sem.at[which])
        await_bytes(ref.at[pl.ds(0, SLOTS - CAP), :], ret_send.at[which])
    for copy in x_copies:
        copy.wait_send()
    for copy in p_copies.values():
        copy.wait_send()
    m2.wait_send()
    for copy in rf_copies:
        copy.wait_send()
    down.wait_send()
    up.wait_send()
    m0.wait_send()
    to_partner.wait_send()
    for copy in z_copies:
        copy.wait_send()
    await_bytes(rt_v.at[pl.ds(0, SP - 1)], rt_send.at[0])


def flush_kernel(*refs):
    count = (len(refs) - 1) // 2
    sems = refs[-1]
    copies = []
    for i in range(count):
        src, dst = refs[i], refs[count + i]
        pieces = 4 if i >= count - 3 else 1
        rows = src.shape[0] // pieces
        for p in range(pieces):
            part = pl.ds(p * rows, rows)
            copies.append(pltpu.make_async_copy(src.at[part, :], dst.at[part, :], sems.at[i, p]))
    for copy in copies:
        copy.start()
    for copy in copies:
        copy.wait()


def per_device(
    out_grad, route_ids, route_weight, expert_inputs, gate_weight, up_weight, down_weight,
    out_gate, in_gate, values, conv_out, conv_taps, proj_weight,
):
    sds = jax.ShapeDtypeStruct
    hbm = pl.BlockSpec(memory_space=pltpu.HBM)
    vm = pltpu.VMEM
    dma = pltpu.SemaphoreType.DMA
    act = (TOK, CH)
    vmem = pl.BlockSpec(memory_space=pltpu.VMEM)
    shapes = [
        sds(act, BF), sds(act, BF), sds(act, BF), sds(act, BF), sds((ROWS, CH), F32),
        sds((TP * CH, HID), BF), sds((TP * CH, HID), BF), sds((HID, TP * CH), BF),
    ]
    outs = pl.pallas_call(
        layer_kernel,
        in_specs=[hbm] * 13,
        out_specs=[vmem] * 8,
        out_shape=[vm(o.shape, o.dtype) for o in shapes],
        scratch_shapes=[
            vm((2, TOK), jnp.int32), vm((2, TOK), F32), vm(act, BF), vm((SLOTS, TP * CH), BF),
            vm((TP * CH, 2 * HID), BF), vm((HID, TP * CH), BF), vm(act, BF), vm(act, BF), vm(act, BF),
            vm(act, BF), vm((3, CH), BF), vm((TP * CH, CH), BF),
            vm(act, BF), vm((SLOTS, TOK), BF), vm((SLOTS, TOK), F32), vm((SLOTS, CH), BF),
            vm((SLOTS, CH), BF), vm((TP, SLOTS, CH), BF), vm((SLOTS, HID), F32), vm((SLOTS, HID), F32),
            vm((SLOTS, HID), BF), vm((SLOTS, 2 * HID), BF),
            vm((TP, SLOTS, CH), BF), vm((2, SLOTS, CH), BF), vm((SLOTS, CH), BF), vm((SLOTS, CH), BF),
            vm((SLOTS, CH), BF), vm(act, BF), vm(act, BF), vm(act, BF), vm(act, BF),
            vm((TP,) + act, BF), vm(act, BF), vm((16, CH), BF), vm((16, CH), BF),
            vm((C, Z, Y) + act, BF), vm((TP, GROUP, ROWS, TOK), BF), vm((SP, ROWS, TOK), BF),
            dma((13,)), dma((2,)), dma((2,)), dma((Z,)), dma((Z,)), dma((2, Z)), dma((2, Z)),
            dma((2, Z)), dma((2, Z)), dma((2,)), dma((2,)), dma((2,)), dma((2,)), dma((2,)), dma((2,)),
            dma((4,)), dma((4, 4)), dma((4, 4)), dma((2,)), dma((1,)), dma((Z,)),
        ],
        compiler_params=pltpu.CompilerParams(
            collective_id=0, has_side_effects=True, vmem_limit_bytes=52428800
        ),
    )(
        route_ids.T, route_weight.T, out_grad, expert_inputs[0], gate_weight[0], up_weight[0],
        down_weight[0], out_gate, in_gate, values, conv_out, conv_taps, proj_weight,
    )
    resid, ogg, igg, vg, proj, gate_grad, up_grad, down_grad = pl.pallas_call(
        flush_kernel,
        in_specs=[vmem] * 8,
        out_specs=[hbm] * 8,
        out_shape=shapes,
        scratch_shapes=[dma((8, 4))],
        compiler_params=pltpu.CompilerParams(vmem_limit_bytes=1024 * 1024),
    )(*outs)
    return resid, ogg, igg, vg, proj, gate_grad[None], up_grad[None], down_grad[None]


def solution(mesh):
    return jax.shard_map(
        per_device,
        mesh=mesh,
        in_specs=(
            P("sp", "tp"), P("sp", None), P("sp", None), P("sp", None, None), P("sp", None, "tp"),
            P("sp", None, "tp"), P("sp", "tp", None), P("sp", "tp"), P("sp", "tp"), P("sp", "tp"),
            P("sp", "tp"), P(None, "tp"), P(None, "tp"),
        ),
        out_specs=(
            P("sp", "tp"), P("sp", "tp"), P("sp", "tp"), P("sp", "tp"), P("sp", "tp"),
            P("sp", None, "tp"), P("sp", None, "tp"), P("sp", "tp", None),
        ),
        check_vma=False,
    )
```

time: 99.7 us -> 69.1 us (0.69); the launches traced: 98 us -> 68.7 us
  Pallas kernels: 88.7 us -> 68.1 us
  local copies, waits for them, and re-layouts: 8.64 us -> 0 us
    pallas_call x2, Pallas kernels: 88.7 us -> 68.1 us  [the longest x1 64 us: per_device(): pl.pallas_call(layer_kernel, in_specs=[hbm] * 13, out_specs=[vmem] * 8, o...]
    unnamed x16 -> x0, local copies, waits for them, and re-layouts: 8.64 us -> none
where the time goes in v2:
time: 69.1 us; the launch traced here: 68.7 us
  Pallas kernels  68.1 us (99%)
    pallas_call x1, Pallas kernels, per_device(): pl.pallas_call(layer_kernel, in_specs=[hbm] * 13, out_specs=[vmem] * 8, o...  64 us
    pallas_call x1, Pallas kernels, per_device(): pl.pallas_call(flush_kernel, in_specs=[vmem] * 8, out_specs=[hbm] * 8, ou...  4.09 us

profile of v2, /device:TPU:0, one launch (start us, length us, event | category | flops | bytes accessed | tf_op | source)
XLA Modules:
  0.0 68.7 jit_solution(15130877240838419792)
XLA Ops:
  0.6 64.0 %shard_map.188 = (bf16[128,512]{1,0:T(8,128)(2,1)S(1)}, bf16[128,512]{1,0:T(8,128)(2,1)S(1)}, bf16[128,512]{1,0:T(8,128)(2,1)S(1)}, bf16[128,512]{1,0:T(8,128)(2...) custom-call(s32[2,128]{1,0:T(2,128)} %bitcast.13, ...), custom_call_target="tpu_custom_call" | custom-call | tf_op jit(solution)/shard_map/pallas_call | solution.py:547
  64.6 4.1 %shard_map.189 = (bf16[128,512]{1,0:T(8,128)(2,1)}, bf16[128,512]{1,0:T(8,128)(2,1)}, bf16[128,512]{1,0:T(8,128)(2,1)}, bf16[128,512]{1,0:T(8,128)(2,1)}, f32[64...) custom-call(bf16[128,512]{1,0:T(8,128)(2,1)S(1)} %get-tuple-element.24.refs_0_, ...), custom_call_target="tpu_custom_call" | custom-call | tf_op jit(solution)/shard_map/pallas_call | solution.py:574

commit v3 on v2

--- a/solution.py
+++ b/solution.py
@@ -61,21 +61,34 @@
         copy.start()
         return copy
 
-    loads = [
-        load(0, ids_hbm, ids_v),
-        load(1, w_hbm, w_v),
-        load(2, og_hbm, og_v),
-        load(3, inp_hbm, inp_v),
-        load(4, gw_hbm, gu_v.at[:, pl.ds(0, HID)]),
-        load(5, uw_hbm, gu_v.at[:, pl.ds(HID, HID)]),
-        load(6, dw_hbm, dw_v),
-        load(7, gate_hbm, gate_v),
-        load(8, conv_hbm, conv_v),
-        load(9, pw_hbm, pw_v),
-        load(10, ing_hbm, ing_v),
-        load(11, val_hbm, val_v),
-        load(12, taps_hbm, taps_v),
-    ]
+    def blocks(i, pairs):
+        for j in range(TP):
+            for src, dst in pairs(at(lax.rem(x + j, TP), CH), pl.ds(j * CH, CH)):
+                load(i, src, dst)
+
+    loads = {
+        0: load(0, ids_hbm, ids_v),
+        1: load(1, w_hbm, w_v),
+        2: load(2, og_hbm, og_v),
+        7: load(7, gate_hbm, gate_v),
+        8: load(8, conv_hbm, conv_v),
+    }
+    blocks(3, lambda theirs, ours: [(inp_hbm.at[:, theirs], inp_v.at[:, ours])])
+    blocks(4, lambda theirs, ours: [
+        (gw_hbm.at[theirs, :], gu_v.at[ours, pl.ds(0, HID)]),
+        (uw_hbm.at[theirs, :], gu_v.at[ours, pl.ds(HID, HID)]),
+    ])
+    blocks(6, lambda theirs, ours: [(dw_hbm.at[:, theirs], dw_v.at[:, ours])])
+    loads |= {
+        9: load(9, pw_hbm, pw_v),
+        10: load(10, ing_hbm, ing_v),
+        11: load(11, val_hbm, val_v),
+        12: load(12, taps_hbm, taps_v),
+    }
+
+    def await_bytes(ref, sem):
+        pltpu.make_async_copy(ref, ref, sem).wait()
+
 
     barrier = pltpu.get_barrier_semaphore()
 
@@ -135,11 +148,6 @@
 
         lax.fori_loop(0, SLOTS // 256, rows_of, 0)
 
-    with jax.named_scope("w_weights"):
-        loads[3].wait()
-        loads[4].wait()
-        loads[5].wait()
-    hidden_tile(0)
     with jax.named_scope("w_barrier"):
         pl.semaphore_wait(barrier, SP - 1 + TP - 1)
 
@@ -173,13 +181,11 @@
                 device_id_type=MESH,
             ).start()
 
-    def await_bytes(ref, sem):
-        pltpu.make_async_copy(ref, ref, sem).wait()
-
     def chunk_rows(dz):
         return at(lax.rem(z + dz, Z), CHUNK)
 
-    scatter(out0_v, 0, 0, recv0_sem, (2, 0))
+    scatter(out0_v, 0, 0, recv0_sem, (0,))
+    scatter(out0_v, 0, 0, recv0_sem, (2,))
     scatter(out0_v, 0, 0, recv0_sem, (1, 3))
 
     x_copies = []
@@ -240,6 +246,10 @@
             z_copies.append(copy)
 
     spread(0)
+    with jax.named_scope("w_weights"):
+        await_bytes(inp_v, ld_sem.at[3])
+        await_bytes(gu_v, ld_sem.at[4])
+    hidden_tile(0)
     hidden_tile(1)
     forward(0)
     with jax.named_scope("w_ogopp"):
@@ -252,7 +262,7 @@
     scatter(out2_v, 2, 1, recv2_sem, (1, 3))
     forward(2)
     forward(3)
-    loads[6].wait()
+    await_bytes(dw_v, ld_sem.at[6])
 
     p_copies = {}
 
@@ -293,16 +303,14 @@
             with jax.named_scope(f"w_x{k}"):
                 x_copies[2 * k].wait_recv()
                 x_copies[2 * k + 1].wait_recv()
-        d_hidden = None
-        for j in range(TP):
-            term = mm(rows_pair(r_v.at[j], halves), dw_v[:, at(lax.rem(x + j, TP), CH)], (1, 1))
-            d_hidden = term if d_hidden is None else d_hidden + term
+        left = jnp.concatenate([rows_pair(r_v.at[j], halves) for j in range(TP)], axis=1)
+        d_hidden = mm(left, dw_v[...], (1, 1))
         if ks[0] == 0:
             spread(2)
         put_pair(dgu_v.at[:, pl.ds(0, HID)], halves, (d_hidden * rows_pair(a_v, halves)).astype(BF))
         put_pair(dgu_v.at[:, pl.ds(HID, HID)], halves, (d_hidden * rows_pair(s_v, halves)).astype(BF))
         for j in (1, 3, 2, 0):
-            part = mm(rows_pair(dgu_v, halves), gu_v[at(lax.rem(x + j, TP), CH), :], (1, 1))
+            part = mm(rows_pair(dgu_v, halves), gu_v[j * CH : (j + 1) * CH, :], (1, 1))
             put_pair(p_v.at[j], halves, part.astype(BF))
             if j in (1, 3):
                 way = 0 if j == 1 else 1
@@ -319,11 +327,8 @@
                     p_copies[way, k] = copy
             if j == 2:
                 give_back(p_v.at[2], ret2_v, 1, [ORDER[k] for k in ks])
-                if ks[0] > 0:
-                    spread(3)
-        if ks[0] > 0:
-            finish_own(0)
-            finish_own(1)
+    finish_own(0)
+    finish_own(1)
 
     slot_scale = 1.0 / math.sqrt(SLOTS)
 
@@ -342,6 +347,7 @@
         def tile(n, carry):
             rows = at(n, 256)
             turned = inp_v[:, rows].T
+            rows = at(lax.rem(x + n // 2, TP) * 2 + lax.rem(n, 2), 256)
             gate_grad_v[rows, :] = (mm(turned, dgu_v[:, 0:HID], (1, 0)) * slot_scale).astype(BF)
             up_grad_v[rows, :] = (mm(turned, dgu_v[:, HID : 2 * HID], (1, 0)) * slot_scale).astype(BF)
             return carry
@@ -350,8 +356,84 @@
 
     finish_own(2)
     finish_own(3)
+    spread(3)
+
+    def await_returned(ref, which):
+        with jax.named_scope(f"w_ret{which}"):
+            await_bytes(ref.at[pl.ds(0, SLOTS - CAP), :], ret_recv.at[which])
+
+    def to_opposite(src, dst, sem):
+        copy = pltpu.make_async_remote_copy(
+            src, dst, sem.at[0], sem.at[1], device_id=(sp, xo), device_id_type=MESH
+        )
+        copy.start()
+        return copy
+
+    await_returned(ret2_v, 1)
+    m2_v[...] = mm(disp_v[...], ret2_v[...], (0, 0)).astype(BF)
+    m2 = to_opposite(m2_v, r2_v, m2_sem)
     with jax.named_scope("g_gate"):
         gate_tiles(0, 4)
+    await_returned(ret0_v, 0)
+    moe = mm(disp_v[...], ret0_v[...], (0, 0))
+    m0_v[...] = moe.astype(BF)
+    sides = (west, east)
+    m0 = [to_opposite(m0_v.at[:, cols], rm0_v.at[:, cols], m0_sem.at[h]) for h, cols in enumerate(sides)]
+    with jax.named_scope("w_m2"):
+        m2.wait_recv()
+    own = (og_v[...].astype(F32) + moe + r2_v[...].astype(F32)).astype(BF)
+    rf_v[0] = own
+    rf_copies = {}
+    for h, cols in enumerate(sides):
+        for there, landing in ((xp, 3), (xm, 1)):
+            copy = pltpu.make_async_remote_copy(
+                rf_v.at[0, :, cols],
+                rf_v.at[landing, :, cols],
+                rf_send.at[landing // 2, h],
+                rf_recv.at[landing // 2, h],
+                device_id=(sp, there),
+                device_id_type=MESH,
+            )
+            copy.start()
+            rf_copies[landing, h] = copy
+    resid_v[...] = own
+    loads[9].wait()
+
+    def mix_part(j):
+        return mm(rf_v[j], pw_v[at(lax.rem(x + j, TP), CH), :], (1, 0))
+
+    def order_of(cc, zz, yy):
+        return (cc * Z + zz) * Y + yy
+
+    mine = order_of(core, z, y)
+
+    HALF = GROUP // 2
+
+    def share(j, h):
+        block = lax.rem(x + j, TP)
+        turned = rf_v[j, :, h * CH // 2 : (h + 1) * CH // 2].T
+        rft_v[j, h * HALF : (h + 1) * HALF] = turned.reshape(HALF, ROWS, TOK)
+        for dy in (1, 0):
+            for dc in (1, 0):
+                inside = (2 * h + lax.rem(y + dy, 2)) * C + lax.rem(core + dc, C)
+                there = block * GROUP + inside
+
+                @pl.when(there != sp)
+                def _():
+                    pltpu.make_async_remote_copy(
+                        rft_v.at[j, inside],
+                        rt_v.at[mine],
+                        rt_send.at[0],
+                        rt_recv.at[lax.rem(z - block + Z, Z)],
+                        device_id=(there, x),
+                        device_id_type=MESH,
+                    ).start()
+
+    share(0, 0)
+    share(0, 1)
+    mix = mix_part(0)
+    with jax.named_scope("g_gate2"):
+        gate_tiles(4, 8)
     with jax.named_scope("w_spread4"):
         for copy in z_copies[-4:]:
             copy.wait_recv()
@@ -360,83 +442,19 @@
         device_id=(partner, x), device_id_type=MESH,
     )
     to_partner.start()
-
-    def await_returned(ref, which):
-        with jax.named_scope(f"w_ret{which}"):
-            await_bytes(ref.at[pl.ds(0, SLOTS - CAP), :], ret_recv.at[which])
-
-    def to_opposite(src, dst, sem):
-        copy = pltpu.make_async_remote_copy(
-            src, dst, sem.at[0], sem.at[1], device_id=(sp, xo), device_id_type=MESH
-        )
-        copy.start()
-        return copy
-
-    await_returned(ret2_v, 1)
-    m2_v[...] = mm(disp_v[...], ret2_v[...], (0, 0)).astype(BF)
-    m2 = to_opposite(m2_v, r2_v, m2_sem)
-    await_returned(ret0_v, 0)
-    moe = mm(disp_v[...], ret0_v[...], (0, 0))
-    m0_v[...] = moe.astype(BF)
-    m0 = to_opposite(m0_v, rm0_v, m0_sem)
-    with jax.named_scope("w_m2"):
-        m2.wait_recv()
-    own = (og_v[...].astype(F32) + moe + r2_v[...].astype(F32)).astype(BF)
-    rf_v[0] = own
-    rf_copies = []
-    for i, (there, landing) in enumerate(((xp, 3), (xm, 1))):
-        copy = pltpu.make_async_remote_copy(
-            rf_v.at[0],
-            rf_v.at[landing],
-            rf_send.at[i],
-            rf_recv.at[i],
-            device_id=(sp, there),
-            device_id_type=MESH,
-        )
-        copy.start()
-        rf_copies.append(copy)
-    resid_v[...] = own
-    loads[9].wait()
-
-    def mix_part(j):
-        return mm(rf_v[j], pw_v[at(lax.rem(x + j, TP), CH), :], (1, 0))
-
-    def order_of(cc, zz, yy):
-        return (cc * Z + zz) * Y + yy
-
-    mine = order_of(core, z, y)
-
-    def share(j):
-        block = lax.rem(x + j, TP)
-        rft_v[j] = rf_v[j].T.reshape(GROUP, ROWS, TOK)
-
-        for there in plane(block, False):
-            inside = lax.rem(there, GROUP)
-
-            @pl.when(there != sp)
-            def _():
-                pltpu.make_async_remote_copy(
-                    rft_v.at[j, inside],
-                    rt_v.at[mine],
-                    rt_send.at[0],
-                    rt_recv.at[lax.rem(z - block + Z, Z)],
-                    device_id=(there, x),
-                    device_id_type=MESH,
-                ).start()
-
-    share(0)
-    mix = mix_part(0)
-    with jax.named_scope("g_gate2"):
-        gate_tiles(4, 8)
-    for j, i in ((3, 0), (1, 1)):
-        with jax.named_scope(f"w_rf{j}"):
-            rf_copies[i].wait_recv()
-        share(j)
+    for h, cols in enumerate(sides):
+        for j in (3, 1):
+            with jax.named_scope(f"w_rf{j}_{h}"):
+                rf_copies[j, h].wait_recv()
+            share(j, h)
+        with jax.named_scope(f"w_rf2_{h}"):
+            m0[h].wait_recv()
+        other = ogopp_v[:, cols].astype(F32) + rm0_v[:, cols].astype(F32) + m2_v[:, cols].astype(F32)
+        rf_v[2, :, cols] = other.astype(BF)
+        if h == 0:
+            share(2, 0)
+    for j in (3, 1, 2):
         mix = mix + mix_part(j)
-    with jax.named_scope("w_rf2"):
-        m0.wait_recv()
-    rf_v[2] = (ogopp_v[...].astype(F32) + rm0_v[...].astype(F32) + m2_v[...].astype(F32)).astype(BF)
-    mix = mix + mix_part(2)
     ogg_v[...] = (mix * conv_vals).astype(BF)
     cg_v[...] = (mix * gate_vals).astype(BF)
     down = pltpu.make_async_remote_copy(
@@ -449,7 +467,7 @@
     )
     down.start()
     up.start()
-    share(2)
+    share(2, 1)
     rt_v[mine] = rft_v[lax.rem(z - x + TP, TP), inner]
     with jax.named_scope("g_down"):
         down_tiles(0, HID // 256)
@@ -502,11 +520,12 @@
     for copy in p_copies.values():
         copy.wait_send()
     m2.wait_send()
-    for copy in rf_copies:
+    for copy in rf_copies.values():
         copy.wait_send()
     down.wait_send()
     up.wait_send()
-    m0.wait_send()
+    for copy in m0:
+        copy.wait_send()
     to_partner.wait_send()
     for copy in z_copies:
         copy.wait_send()
@@ -561,7 +580,7 @@
             vm((TP,) + act, BF), vm(act, BF), vm((16, CH), BF), vm((16, CH), BF),
             vm((C, Z, Y) + act, BF), vm((TP, GROUP, ROWS, TOK), BF), vm((SP, ROWS, TOK), BF),
             dma((13,)), dma((2,)), dma((2,)), dma((Z,)), dma((Z,)), dma((2, Z)), dma((2, Z)),
-            dma((2, Z)), dma((2, Z)), dma((2,)), dma((2,)), dma((2,)), dma((2,)), dma((2,)), dma((2,)),
+            dma((2, Z)), dma((2, Z)), dma((2,)), dma((2,)), dma((2,)), dma((2, 2)), dma((2, 2)), dma((2, 2)),
             dma((4,)), dma((4, 4)), dma((4, 4)), dma((2,)), dma((1,)), dma((Z,)),
         ],
         compiler_params=pltpu.CompilerParams(

time: 69.1 us -> 63.7 us (0.922)
  Pallas kernels: 68.1 us -> 63 us
    pallas_call x1, Pallas kernels: 64 us -> 58.9 us  [per_device(): pl.pallas_call(layer_kernel, in_specs=[hbm] * 13, out_specs=[vmem] * 8, o...]
where the time goes in v3:
time: 63.7 us; the launch traced here: 63.6 us
  Pallas kernels  63 us (99%)
  between operations  0.65 us (1%)
    pallas_call x1, Pallas kernels, per_device(): pl.pallas_call(layer_kernel, in_specs=[hbm] * 13, out_specs=[vmem] * 8, o...  58.9 us
    pallas_call x1, Pallas kernels, per_device(): pl.pallas_call(flush_kernel, in_specs=[vmem] * 8, out_specs=[hbm] * 8, ou...  4.09 us

profile of v3, /device:TPU:0, one launch (start us, length us, event | category | flops | bytes accessed | tf_op | source)
XLA Modules:
  0.0 63.6 jit_solution(2381121113832291244)
XLA Ops:
  0.6 58.9 %shard_map.188 = (bf16[128,512]{1,0:T(8,128)(2,1)S(1)}, bf16[128,512]{1,0:T(8,128)(2,1)S(1)}, bf16[128,512]{1,0:T(8,128)(2,1)S(1)}, bf16[128,512]{1,0:T(8,128)(2...) custom-call(s32[2,128]{1,0:T(2,128)} %bitcast.13, ...), custom_call_target="tpu_custom_call" | custom-call | tf_op jit(solution)/shard_map/pallas_call | solution.py:566
  59.5 4.1 %shard_map.189 = (bf16[128,512]{1,0:T(8,128)(2,1)}, bf16[128,512]{1,0:T(8,128)(2,1)}, bf16[128,512]{1,0:T(8,128)(2,1)}, bf16[128,512]{1,0:T(8,128)(2,1)}, f32[64...) custom-call(bf16[128,512]{1,0:T(8,128)(2,1)S(1)} %get-tuple-element.24.refs_0_, ...), custom_call_target="tpu_custom_call" | custom-call | tf_op jit(solution)/shard_map/pallas_call | solution.py:593

commit v4 on v3

--- a/solution.py
+++ b/solution.py
@@ -70,9 +70,11 @@
         0: load(0, ids_hbm, ids_v),
         1: load(1, w_hbm, w_v),
         2: load(2, og_hbm, og_v),
-        7: load(7, gate_hbm, gate_v),
-        8: load(8, conv_hbm, conv_v),
     }
+    load(7, gate_hbm, gate_v)
+    load(7, conv_hbm, conv_v)
+    load(7, ing_hbm, ing_v)
+    load(7, val_hbm, val_v)
     blocks(3, lambda theirs, ours: [(inp_hbm.at[:, theirs], inp_v.at[:, ours])])
     blocks(4, lambda theirs, ours: [
         (gw_hbm.at[theirs, :], gu_v.at[ours, pl.ds(0, HID)]),
@@ -80,10 +82,8 @@
     ])
     blocks(6, lambda theirs, ours: [(dw_hbm.at[:, theirs], dw_v.at[:, ours])])
     loads |= {
-        9: load(9, pw_hbm, pw_v),
-        10: load(10, ing_hbm, ing_v),
-        11: load(11, val_hbm, val_v),
-        12: load(12, taps_hbm, taps_v),
+        9: load(5, pw_hbm, pw_v),
+        12: load(8, taps_hbm, taps_v),
     }
 
     def await_bytes(ref, sem):
@@ -184,34 +184,53 @@
     def chunk_rows(dz):
         return at(lax.rem(z + dz, Z), CHUNK)
 
-    scatter(out0_v, 0, 0, recv0_sem, (0,))
+    r_v[0, at(sp, CAP), :] = out0_v[at(sp, CAP), :]
+    for dy in (1, 3, 0, 2):
+        for dc in (1, 0) if dy else (1,):
+            there = (z * Y + lax.rem(y + dy, Y)) * C + lax.rem(core + dc, C)
+            pltpu.make_async_remote_copy(
+                out0_v.at[at(there, CAP), :],
+                r_v.at[0, at(sp, CAP), :],
+                disp_sem.at[0],
+                recv0_sem.at[Z if dy == 2 else 0],
+                device_id=(there, x),
+                device_id_type=MESH,
+            ).start()
     scatter(out0_v, 0, 0, recv0_sem, (2,))
     scatter(out0_v, 0, 0, recv0_sem, (1, 3))
-
-    x_copies = []
 
     def await_group(block, dz, recv_sem):
         count = CHUNK - CAP if dz == 0 else CHUNK
         with jax.named_scope(f"w_group{block}_{dz}"):
             await_bytes(r_v.at[block, pl.ds(0, count), :], recv_sem.at[dz])
 
-    def forward(k):
-        dz = ORDER[k]
-        await_group(0, dz, recv0_sem)
+    def forward_rows(k, rows):
         for way, (there, landing) in enumerate(((xp, 3), (xm, 1))):
             copy = pltpu.make_async_remote_copy(
-                r_v.at[0, chunk_rows(dz), :],
-                r_v.at[landing, chunk_rows(dz), :],
-                x_send.at[way, k],
-                x_recv.at[way, k],
+                r_v.at[0, rows, :],
+                r_v.at[landing, rows, :],
+                x_send.at[0],
+                x_recv.at[k],
                 device_id=(sp, there),
                 device_id_type=MESH,
             )
             copy.start()
-            x_copies.append(copy)
-
-    loads[7].wait()
-    loads[8].wait()
+
+    def forward_first():
+        near = C * CAP
+        with jax.named_scope("w_group0_0"):
+            await_bytes(r_v.at[0, pl.ds(0, 3 * near - CAP), :], recv0_sem.at[0])
+        for dy in (0, 1, 3):
+            forward_rows(0, at(z * Y + lax.rem(y + dy, Y), near))
+        with jax.named_scope("w_group0_far"):
+            await_bytes(r_v.at[0, pl.ds(0, near), :], recv0_sem.at[Z])
+        forward_rows(0, at(z * Y + lax.rem(y + 2, Y), near))
+
+    def forward(k):
+        await_group(0, ORDER[k], recv0_sem)
+        forward_rows(k, chunk_rows(ORDER[k]))
+
+    await_bytes(rf_v, ld_sem.at[7])
     gate_vals = gate_v[...].astype(F32)
     conv_vals = conv_v[...].astype(F32)
     zall_v[core, z, y] = (gate_vals * conv_vals).astype(BF)
@@ -221,7 +240,11 @@
     west, east = pl.ds(0, CH // 2), pl.ds(CH // 2, CH // 2)
     low, high, full = pl.ds(0, TOK // 2), pl.ds(TOK // 2, TOK // 2), pl.ds(0, TOK)
     every = pl.ds(0, Z)
-    z_copies = []
+
+    def spread_arrived(phase):
+        rows = (2 * TOK, TOK, 8 * TOK, 4 * TOK)[phase]
+        with jax.named_scope(f"w_spread{phase + 1}"):
+            await_bytes(r_v.at[pl.ds(0, rows // TOK), pl.ds(0, TOK), :] if rows <= 2 * TOK else r_v.at[pl.ds(0, 2), pl.ds(0, rows // 2), :], za_recv.at[phase])
 
     def spread(phase):
         steps = (
@@ -233,17 +256,14 @@
         along_y, along_z = ((z, yp), (z, ym)), ((zp, y), (zm, y))
         theres = along_y + along_z if phase < 2 else along_z + along_y
         if phase > 0:
-            with jax.named_scope(f"w_spread{phase}"):
-                for copy in z_copies[-4:]:
-                    copy.wait_recv()
-        for way, ((bz, by, rows, cols), (tz, ty)) in enumerate(zip(steps, theres)):
+            spread_arrived(phase - 1)
+        for (bz, by, rows, cols), (tz, ty) in zip(steps, theres):
             part = zall_v.at[core, bz, by, rows, cols]
             copy = pltpu.make_async_remote_copy(
-                part, part, za_send.at[phase, way], za_recv.at[phase, way],
+                part, part, za_send.at[0], za_recv.at[phase],
                 device_id=((tz * Y + ty) * C + core, x), device_id_type=MESH,
             )
             copy.start()
-            z_copies.append(copy)
 
     spread(0)
     with jax.named_scope("w_weights"):
@@ -251,7 +271,7 @@
         await_bytes(gu_v, ld_sem.at[4])
     hidden_tile(0)
     hidden_tile(1)
-    forward(0)
+    forward_first()
     with jax.named_scope("w_ogopp"):
         ogopp.wait_recv()
     dispatch(ogopp_v, out2_v)
@@ -264,12 +284,13 @@
     forward(3)
     await_bytes(dw_v, ld_sem.at[6])
 
-    p_copies = {}
-
     def give_back(src_ref, dst_ref, which, dzs):
         if 0 in dzs:
             dst_ref[at(sp, CAP), :] = src_ref[at(sp, CAP), :]
-        for _, there in interleaved(dzs, 1):
+        give_rows(src_ref, dst_ref, which, [there for _, there in interleaved(dzs, 1)])
+
+    def give_rows(src_ref, dst_ref, which, theres):
+        for there in theres:
             pltpu.make_async_remote_copy(
                 src_ref.at[at(there, CAP), :],
                 dst_ref.at[at(sp, CAP), :],
@@ -279,30 +300,51 @@
                 device_id_type=MESH,
             ).start()
 
+    HALF = GROUP // 2
+
+    def half_plane(zz, h):
+        return [
+            (zz * Y + 2 * h + lax.rem(y + dy, 2)) * C + lax.rem(core + dc, C)
+            for dy in (1, 0)
+            for dc in (1, 0)
+        ]
+
+    def pieces(k):
+        if k < 2:
+            return [(k, chunk_rows(ORDER[k]), CHUNK)]
+        h = k - 2
+        return [
+            (2 * k - 2 + i, at(lax.rem(z + dz, Z) * 2 + h, CHUNK // 2), CHUNK // 2)
+            for i, dz in enumerate(ORDER[2:])
+        ]
+
     def finish_own(k):
-        dz = ORDER[k]
-        rows = chunk_rows(dz)
         with jax.named_scope(f"w_part{k}"):
-            for way in range(2):
-                p_copies[way, k].wait_recv()
-        total = p_v[0, rows, :].astype(F32) + rp_v[0, rows, :].astype(F32) + rp_v[1, rows, :].astype(F32)
-        b0_v[rows, :] = total.astype(BF)
-        give_back(b0_v, ret0_v, 0, (dz,))
+            await_bytes(rp_v.at[:, pl.ds(0, CHUNK), :], pn_recv.at[k])
+        for _, rows, _ in pieces(k):
+            total = p_v[0, rows, :].astype(F32) + rp_v[0, rows, :].astype(F32) + rp_v[1, rows, :].astype(F32)
+            b0_v[rows, :] = total.astype(BF)
+        if k < 2:
+            give_back(b0_v, ret0_v, 0, (ORDER[k],))
+        else:
+            lists = [half_plane(lax.rem(z + dz, Z), k - 2) for dz in ORDER[2:]]
+            give_rows(b0_v, ret0_v, 0, [there for pair in zip(*lists) for there in pair])
 
     def rows_pair(ref, halves):
-        return jnp.concatenate([ref[rows, :] for rows in halves], axis=0)
+        return jnp.concatenate([ref[rows, :] for _, rows, _ in halves], axis=0)
 
     def put_pair(ref, halves, value):
-        for h, rows in enumerate(halves):
-            ref[rows, :] = value[h * CHUNK : (h + 1) * CHUNK, :]
+        start = 0
+        for _, rows, size in halves:
+            ref[rows, :] = value[start : start + size, :]
+            start += size
 
     for ks in ((0, 1), (2, 3)):
-        halves = [chunk_rows(ORDER[k]) for k in ks]
+        halves = [piece for k in ks for piece in pieces(k)]
         for k in ks:
             await_group(2, ORDER[k], recv2_sem)
             with jax.named_scope(f"w_x{k}"):
-                x_copies[2 * k].wait_recv()
-                x_copies[2 * k + 1].wait_recv()
+                await_bytes(r_v.at[pl.ds(0, 2), pl.ds(0, CHUNK), :], x_recv.at[k])
         left = jnp.concatenate([rows_pair(r_v.at[j], halves) for j in range(TP)], axis=1)
         d_hidden = mm(left, dw_v[...], (1, 1))
         if ks[0] == 0:
@@ -314,17 +356,16 @@
             put_pair(p_v.at[j], halves, part.astype(BF))
             if j in (1, 3):
                 way = 0 if j == 1 else 1
-                for k, rows in zip(ks, halves):
+                for i, rows, _ in halves:
                     copy = pltpu.make_async_remote_copy(
                         p_v.at[j, rows, :],
                         rp_v.at[way, rows, :],
-                        pn_send.at[way, k],
-                        pn_recv.at[way, k],
+                        pn_send.at[0],
+                        pn_recv.at[i if i < 2 else i // 2 + 1],
                         device_id=(sp, xp if j == 1 else xm),
                         device_id_type=MESH,
                     )
                     copy.start()
-                    p_copies[way, k] = copy
             if j == 2:
                 give_back(p_v.at[2], ret2_v, 1, [ORDER[k] for k in ks])
     finish_own(0)
@@ -362,40 +403,56 @@
         with jax.named_scope(f"w_ret{which}"):
             await_bytes(ref.at[pl.ds(0, SLOTS - CAP), :], ret_recv.at[which])
 
-    def to_opposite(src, dst, sem):
+    def to_opposite(src, dst, send_sem, recv_sem):
         copy = pltpu.make_async_remote_copy(
-            src, dst, sem.at[0], sem.at[1], device_id=(sp, xo), device_id_type=MESH
+            src, dst, send_sem, recv_sem, device_id=(sp, xo), device_id_type=MESH
         )
         copy.start()
         return copy
 
     await_returned(ret2_v, 1)
     m2_v[...] = mm(disp_v[...], ret2_v[...], (0, 0)).astype(BF)
-    m2 = to_opposite(m2_v, r2_v, m2_sem)
+    m2 = to_opposite(m2_v, r2_v, m2_sem.at[0], m2_sem.at[1])
     with jax.named_scope("g_gate"):
         gate_tiles(0, 4)
     await_returned(ret0_v, 0)
     moe = mm(disp_v[...], ret0_v[...], (0, 0))
     m0_v[...] = moe.astype(BF)
-    sides = (west, east)
-    m0 = [to_opposite(m0_v.at[:, cols], rm0_v.at[:, cols], m0_sem.at[h]) for h, cols in enumerate(sides)]
+    m0 = {}
+
+    def lanes(s):
+        return at(lax.rem(y + s, Y), TOK)
+
+    def send_m0(s):
+        m0[s] = to_opposite(m0_v.at[:, lanes(s)], rm0_v.at[:, lanes(s)], m0_sem.at[Y], m0_sem.at[s])
+
+    send_m0(2)
+    send_m0(0)
     with jax.named_scope("w_m2"):
         m2.wait_recv()
     own = (og_v[...].astype(F32) + moe + r2_v[...].astype(F32)).astype(BF)
     rf_v[0] = own
     rf_copies = {}
-    for h, cols in enumerate(sides):
+
+    def send_rf(s):
         for there, landing in ((xp, 3), (xm, 1)):
             copy = pltpu.make_async_remote_copy(
-                rf_v.at[0, :, cols],
-                rf_v.at[landing, :, cols],
-                rf_send.at[landing // 2, h],
-                rf_recv.at[landing // 2, h],
+                rf_v.at[0, :, lanes(s)],
+                rf_v.at[landing, :, lanes(s)],
+                rf_send.at[0],
+                rf_recv.at[landing // 2, s],
                 device_id=(sp, there),
                 device_id_type=MESH,
             )
             copy.start()
-            rf_copies[landing, h] = copy
+            rf_copies[landing, s] = copy
+
+    send_rf(2)
+    send_rf(0)
+    send_m0(1)
+    send_m0(3)
+    send_rf(1)
+    send_rf(3)
     resid_v[...] = own
     loads[9].wait()
 
@@ -407,52 +464,48 @@
 
     mine = order_of(core, z, y)
 
-    HALF = GROUP // 2
-
-    def share(j, h):
+    def share(j, s):
         block = lax.rem(x + j, TP)
-        turned = rf_v[j, :, h * CH // 2 : (h + 1) * CH // 2].T
-        rft_v[j, h * HALF : (h + 1) * HALF] = turned.reshape(HALF, ROWS, TOK)
-        for dy in (1, 0):
-            for dc in (1, 0):
-                inside = (2 * h + lax.rem(y + dy, 2)) * C + lax.rem(core + dc, C)
-                there = block * GROUP + inside
-
-                @pl.when(there != sp)
-                def _():
-                    pltpu.make_async_remote_copy(
-                        rft_v.at[j, inside],
-                        rt_v.at[mine],
-                        rt_send.at[0],
-                        rt_recv.at[lax.rem(z - block + Z, Z)],
-                        device_id=(there, x),
-                        device_id_type=MESH,
-                    ).start()
-
-    share(0, 0)
-    share(0, 1)
+        across = lax.rem(y + s, Y)
+        rft_v[j, across] = rf_v[j, :, lanes(s)].T.reshape(C, ROWS, TOK)
+        for dc in (1, 0):
+            inside = lax.rem(core + dc, C)
+            there = (block * Y + across) * C + inside
+
+            @pl.when(there != sp)
+            def _():
+                pltpu.make_async_remote_copy(
+                    rft_v.at[j, across, inside],
+                    rt_v.at[mine],
+                    rt_send.at[0],
+                    rt_recv.at[lax.rem(z - block + Z, Z)],
+                    device_id=(there, x),
+                    device_id_type=MESH,
+                ).start()
+
+    for s in (2, 0, 1, 3):
+        share(0, s)
     mix = mix_part(0)
     with jax.named_scope("g_gate2"):
         gate_tiles(4, 8)
-    with jax.named_scope("w_spread4"):
-        for copy in z_copies[-4:]:
-            copy.wait_recv()
+    spread_arrived(3)
     to_partner = pltpu.make_async_remote_copy(
         zall_v.at[core], zall_v.at[core], zd_sem.at[0], zd_sem.at[1],
         device_id=(partner, x), device_id_type=MESH,
     )
     to_partner.start()
-    for h, cols in enumerate(sides):
+    for s in (2, 0, 1, 3):
         for j in (3, 1):
-            with jax.named_scope(f"w_rf{j}_{h}"):
-                rf_copies[j, h].wait_recv()
-            share(j, h)
-        with jax.named_scope(f"w_rf2_{h}"):
-            m0[h].wait_recv()
+            with jax.named_scope(f"w_rf{j}_{s}"):
+                rf_copies[j, s].wait_recv()
+            share(j, s)
+        with jax.named_scope(f"w_rf2_{s}"):
+            m0[s].wait_recv()
+        cols = lanes(s)
         other = ogopp_v[:, cols].astype(F32) + rm0_v[:, cols].astype(F32) + m2_v[:, cols].astype(F32)
         rf_v[2, :, cols] = other.astype(BF)
-        if h == 0:
-            share(2, 0)
+        if s in (2, 0):
+            share(2, s)
     for j in (3, 1, 2):
         mix = mix + mix_part(j)
     ogg_v[...] = (mix * conv_vals).astype(BF)
@@ -468,9 +521,17 @@
     down.start()
     up.start()
     share(2, 1)
-    rt_v[mine] = rft_v[lax.rem(z - x + TP, TP), inner]
+    share(2, 3)
+    rt_v[mine] = rft_v[lax.rem(z - x + TP, TP), y, core]
     with jax.named_scope("g_down"):
         down_tiles(0, HID // 256)
+    ogopp.wait_send()
+    for which, ref in ((0, out0_v), (1, out2_v)):
+        await_bytes(ref.at[pl.ds(0, SLOTS - CAP), :], disp_sem.at[which])
+        await_bytes(ref.at[pl.ds(0, SLOTS - CAP), :], ret_send.at[which])
+    m2.wait_send()
+    await_bytes(r_v.at[pl.ds(0, 2)], x_send.at[0])
+    await_bytes(r_v.at[pl.ds(0, 2)], pn_send.at[0])
     with jax.named_scope("w_zd"):
         to_partner.wait_recv()
 
@@ -488,8 +549,6 @@
 
     proj = proj_group(0) + proj_group(1)
 
-    loads[10].wait()
-    loads[11].wait()
     loads[12].wait()
     with jax.named_scope("w_halo"):
         down.wait_recv()
@@ -511,42 +570,27 @@
     proj = proj + proj_group(2)
     proj_v[...] = proj * (1.0 / math.sqrt(TOK * SP))
 
-    ogopp.wait_send()
-    for which, ref in ((0, out0_v), (1, out2_v)):
-        await_bytes(ref.at[pl.ds(0, SLOTS - CAP), :], disp_sem.at[which])
-        await_bytes(ref.at[pl.ds(0, SLOTS - CAP), :], ret_send.at[which])
-    for copy in x_copies:
-        copy.wait_send()
-    for copy in p_copies.values():
-        copy.wait_send()
-    m2.wait_send()
-    for copy in rf_copies.values():
-        copy.wait_send()
+    await_bytes(r_v.at[:, pl.ds(0, 15 * TOK // TP), :], za_send.at[0])
+    to_partner.wait_send()
+    await_bytes(m0_v, m0_sem.at[Y])
+    await_bytes(rf_v.at[pl.ds(0, 2)], rf_send.at[0])
     down.wait_send()
     up.wait_send()
-    for copy in m0:
-        copy.wait_send()
-    to_partner.wait_send()
-    for copy in z_copies:
-        copy.wait_send()
     await_bytes(rt_v.at[pl.ds(0, SP - 1)], rt_send.at[0])
 
 
 def flush_kernel(*refs):
     count = (len(refs) - 1) // 2
     sems = refs[-1]
-    copies = []
-    for i in range(count):
+    for i in reversed(range(count)):
         src, dst = refs[i], refs[count + i]
         pieces = 4 if i >= count - 3 else 1
         rows = src.shape[0] // pieces
         for p in range(pieces):
             part = pl.ds(p * rows, rows)
-            copies.append(pltpu.make_async_copy(src.at[part, :], dst.at[part, :], sems.at[i, p]))
-    for copy in copies:
-        copy.start()
-    for copy in copies:
-        copy.wait()
+            pltpu.make_async_copy(src.at[part, :], dst.at[part, :], sems.at[i]).start()
+    for i in range(count):
+        pltpu.make_async_copy(refs[i], refs[count + i], sems.at[i]).wait()
 
 
 def per_device(
@@ -578,10 +622,10 @@
             vm((TP, SLOTS, CH), BF), vm((2, SLOTS, CH), BF), vm((SLOTS, CH), BF), vm((SLOTS, CH), BF),
             vm((SLOTS, CH), BF), vm(act, BF), vm(act, BF), vm(act, BF), vm(act, BF),
             vm((TP,) + act, BF), vm(act, BF), vm((16, CH), BF), vm((16, CH), BF),
-            vm((C, Z, Y) + act, BF), vm((TP, GROUP, ROWS, TOK), BF), vm((SP, ROWS, TOK), BF),
-            dma((13,)), dma((2,)), dma((2,)), dma((Z,)), dma((Z,)), dma((2, Z)), dma((2, Z)),
-            dma((2, Z)), dma((2, Z)), dma((2,)), dma((2,)), dma((2,)), dma((2, 2)), dma((2, 2)), dma((2, 2)),
-            dma((4,)), dma((4, 4)), dma((4, 4)), dma((2,)), dma((1,)), dma((Z,)),
+            vm((C, Z, Y) + act, BF), vm((TP, Y, C, ROWS, TOK), BF), vm((SP, ROWS, TOK), BF),
+            dma((9,)), dma((2,)), dma((2,)), dma((Z + 1,)), dma((Z,)), dma((1,)), dma((Z,)),
+            dma((1,)), dma((Z,)), dma((2,)), dma((2,)), dma((2,)), dma((Y + 1,)), dma((1,)), dma((2, Y)),
+            dma((4,)), dma((1,)), dma((4,)), dma((2,)), dma((1,)), dma((Z,)),
         ],
         compiler_params=pltpu.CompilerParams(
             collective_id=0, has_side_effects=True, vmem_limit_bytes=52428800
@@ -595,7 +639,7 @@
         in_specs=[vmem] * 8,
         out_specs=[hbm] * 8,
         out_shape=shapes,
-        scratch_shapes=[dma((8, 4))],
+        scratch_shapes=[dma((8,))],
         compiler_params=pltpu.CompilerParams(vmem_limit_bytes=1024 * 1024),
     )(*outs)
     return resid, ogg, igg, vg, proj, gate_grad[None], up_grad[None], down_grad[None]

time: 63.7 us -> 61.5 us (0.965)
  Pallas kernels: 63 us -> 60.5 us
    pallas_call x1, Pallas kernels: 58.9 us -> 56.7 us  [per_device(): pl.pallas_call(layer_kernel, in_specs=[hbm] * 13, out_specs=[vmem] * 8, o...]
where the time goes in v4:
time: 61.5 us; the launch traced here: 61.2 us
  Pallas kernels  60.5 us (98%)
  between operations  0.65 us (1%)
    pallas_call x1, Pallas kernels, per_device(): pl.pallas_call(layer_kernel, in_specs=[hbm] * 13, out_specs=[vmem] * 8, o...  56.7 us
    pallas_call x1, Pallas kernels, per_device(): pl.pallas_call(flush_kernel, in_specs=[vmem] * 8, out_specs=[hbm] * 8, ou...  3.87 us

profile of v4, /device:TPU:0, one launch (start us, length us, event | category | flops | bytes accessed | tf_op | source)
XLA Modules:
  0.0 61.2 jit_solution(13014126192374761706)
XLA Ops:
  0.6 56.7 %shard_map.188 = (bf16[128,512]{1,0:T(8,128)(2,1)S(1)}, bf16[128,512]{1,0:T(8,128)(2,1)S(1)}, bf16[128,512]{1,0:T(8,128)(2,1)S(1)}, bf16[128,512]{1,0:T(8,128)(2...) custom-call(s32[2,128]{1,0:T(2,128)} %bitcast.13, ...), custom_call_target="tpu_custom_call" | custom-call | tf_op jit(solution)/shard_map/pallas_call | solution.py:610
  57.3 3.9 %shard_map.189 = (bf16[128,512]{1,0:T(8,128)(2,1)}, bf16[128,512]{1,0:T(8,128)(2,1)}, bf16[128,512]{1,0:T(8,128)(2,1)}, bf16[128,512]{1,0:T(8,128)(2,1)}, f32[64...) custom-call(bf16[128,512]{1,0:T(8,128)(2,1)S(1)} %get-tuple-element.24.refs_0_, ...), custom_call_target="tpu_custom_call" | custom-call | tf_op jit(solution)/shard_map/pallas_call | solution.py:637

commit v5 on v4

--- a/solution.py
+++ b/solution.py
@@ -61,16 +61,32 @@
         copy.start()
         return copy
 
+    first_loads = {
+        0: load(0, ids_hbm, ids_v),
+        1: load(1, w_hbm, w_v),
+        2: load(2, og_hbm, og_v),
+    }
+    barrier = pltpu.get_barrier_semaphore()
+
+    def greet(s, t):
+        pl.semaphore_signal(barrier, inc=1, device_id=(s, t), device_id_type=MESH)
+
+    for dz in FAR_FIRST:
+        for dy in FAR_FIRST:
+            for dc in (1, 0):
+                if dz or dy or dc:
+                    chip_there = lax.rem(z + dz, Z) * Y + lax.rem(y + dy, Y)
+                    greet(chip_there * C + lax.rem(core + dc, C), x)
+        if dz == 2:
+            for t in (xo, xp, xm):
+                greet(sp, t)
+
     def blocks(i, pairs):
         for j in range(TP):
             for src, dst in pairs(at(lax.rem(x + j, TP), CH), pl.ds(j * CH, CH)):
                 load(i, src, dst)
 
-    loads = {
-        0: load(0, ids_hbm, ids_v),
-        1: load(1, w_hbm, w_v),
-        2: load(2, og_hbm, og_v),
-    }
+    loads = first_loads
     load(7, gate_hbm, gate_v)
     load(7, conv_hbm, conv_v)
     load(7, ing_hbm, ing_v)
@@ -89,17 +105,6 @@
     def await_bytes(ref, sem):
         pltpu.make_async_copy(ref, ref, sem).wait()
 
-
-    barrier = pltpu.get_barrier_semaphore()
-
-    def greet(i, carry):
-        other = lax.rem(sp + 1 + i, SP)
-        pl.semaphore_signal(barrier, inc=1, device_id=(other, x), device_id_type=MESH)
-        return carry
-
-    lax.fori_loop(0, SP - 1, greet, 0)
-    for t in (xp, xm, xo):
-        pl.semaphore_signal(barrier, inc=1, device_id=(sp, t), device_id_type=MESH)
 
     with jax.named_scope("w_load"):
         loads[0].wait()
@@ -176,7 +181,7 @@
                 out_ref.at[at(there, CAP), :],
                 r_v.at[block, at(sp, CAP), :],
                 disp_sem.at[which],
-                recv_sem.at[dz],
+                recv_sem.at[dz % 2 if block == 2 else dz],
                 device_id=(there, x),
                 device_id_type=MESH,
             ).start()
@@ -210,7 +215,7 @@
                 r_v.at[0, rows, :],
                 r_v.at[landing, rows, :],
                 x_send.at[0],
-                x_recv.at[k],
+                x_recv.at[k // 2],
                 device_id=(sp, there),
                 device_id_type=MESH,
             )
@@ -341,10 +346,11 @@
 
     for ks in ((0, 1), (2, 3)):
         halves = [piece for k in ks for piece in pieces(k)]
-        for k in ks:
-            await_group(2, ORDER[k], recv2_sem)
-            with jax.named_scope(f"w_x{k}"):
-                await_bytes(r_v.at[pl.ds(0, 2), pl.ds(0, CHUNK), :], x_recv.at[k])
+        part = ks[0] // 2
+        with jax.named_scope(f"w_opp{part}"):
+            await_bytes(r_v.at[2, pl.ds(0, 2 * CHUNK - (0 if part else CAP)), :], recv2_sem.at[part])
+        with jax.named_scope(f"w_x{part}"):
+            await_bytes(r_v.at[pl.ds(0, 2), pl.ds(0, 2 * CHUNK), :], x_recv.at[part])
         left = jnp.concatenate([rows_pair(r_v.at[j], halves) for j in range(TP)], axis=1)
         d_hidden = mm(left, dw_v[...], (1, 1))
         if ks[0] == 0:
@@ -397,7 +403,6 @@
 
     finish_own(2)
     finish_own(3)
-    spread(3)
 
     def await_returned(ref, which):
         with jax.named_scope(f"w_ret{which}"):
@@ -413,18 +418,18 @@
     await_returned(ret2_v, 1)
     m2_v[...] = mm(disp_v[...], ret2_v[...], (0, 0)).astype(BF)
     m2 = to_opposite(m2_v, r2_v, m2_sem.at[0], m2_sem.at[1])
+    spread(3)
     with jax.named_scope("g_gate"):
         gate_tiles(0, 4)
     await_returned(ret0_v, 0)
     moe = mm(disp_v[...], ret0_v[...], (0, 0))
     m0_v[...] = moe.astype(BF)
-    m0 = {}
 
     def lanes(s):
         return at(lax.rem(y + s, Y), TOK)
 
     def send_m0(s):
-        m0[s] = to_opposite(m0_v.at[:, lanes(s)], rm0_v.at[:, lanes(s)], m0_sem.at[Y], m0_sem.at[s])
+        to_opposite(m0_v.at[:, lanes(s)], rm0_v.at[:, lanes(s)], m0_sem.at[0], rf_recv.at[s])
 
     send_m0(2)
     send_m0(0)
@@ -432,20 +437,17 @@
         m2.wait_recv()
     own = (og_v[...].astype(F32) + moe + r2_v[...].astype(F32)).astype(BF)
     rf_v[0] = own
-    rf_copies = {}
-
     def send_rf(s):
         for there, landing in ((xp, 3), (xm, 1)):
             copy = pltpu.make_async_remote_copy(
                 rf_v.at[0, :, lanes(s)],
                 rf_v.at[landing, :, lanes(s)],
                 rf_send.at[0],
-                rf_recv.at[landing // 2, s],
+                rf_recv.at[s],
                 device_id=(sp, there),
                 device_id_type=MESH,
             )
             copy.start()
-            rf_copies[landing, s] = copy
 
     send_rf(2)
     send_rf(0)
@@ -488,24 +490,22 @@
     mix = mix_part(0)
     with jax.named_scope("g_gate2"):
         gate_tiles(4, 8)
-    spread_arrived(3)
-    to_partner = pltpu.make_async_remote_copy(
-        zall_v.at[core], zall_v.at[core], zd_sem.at[0], zd_sem.at[1],
-        device_id=(partner, x), device_id_type=MESH,
-    )
-    to_partner.start()
     for s in (2, 0, 1, 3):
-        for j in (3, 1):
-            with jax.named_scope(f"w_rf{j}_{s}"):
-                rf_copies[j, s].wait_recv()
-            share(j, s)
-        with jax.named_scope(f"w_rf2_{s}"):
-            m0[s].wait_recv()
+        with jax.named_scope(f"w_rf_{s}"):
+            await_bytes(rf_v.at[pl.ds(0, 3), :, pl.ds(0, TOK)], rf_recv.at[s])
+        share(3, s)
+        share(1, s)
         cols = lanes(s)
         other = ogopp_v[:, cols].astype(F32) + rm0_v[:, cols].astype(F32) + m2_v[:, cols].astype(F32)
         rf_v[2, :, cols] = other.astype(BF)
-        if s in (2, 0):
-            share(2, s)
+        share(2, s)
+        if s == 2:
+            spread_arrived(3)
+            to_partner = pltpu.make_async_remote_copy(
+                zall_v.at[core], zall_v.at[core], zd_sem.at[0], zd_sem.at[1],
+                device_id=(partner, x), device_id_type=MESH,
+            )
+            to_partner.start()
     for j in (3, 1, 2):
         mix = mix + mix_part(j)
     ogg_v[...] = (mix * conv_vals).astype(BF)
@@ -515,13 +515,11 @@
         device_id=(lax.rem(sp + SP - 1, SP), x), device_id_type=MESH,
     )
     up = pltpu.make_async_remote_copy(
-        cg_v.at[pl.ds(TOK - 16, 16), :], before_v, halo_sem.at[2], halo_sem.at[3],
+        cg_v.at[pl.ds(TOK - 16, 16), :], before_v, halo_sem.at[0], halo_sem.at[1],
         device_id=(lax.rem(sp + 1, SP), x), device_id_type=MESH,
     )
     down.start()
     up.start()
-    share(2, 1)
-    share(2, 3)
     rt_v[mine] = rft_v[lax.rem(z - x + TP, TP), y, core]
     with jax.named_scope("g_down"):
         down_tiles(0, HID // 256)
@@ -551,8 +549,7 @@
 
     loads[12].wait()
     with jax.named_scope("w_halo"):
-        down.wait_recv()
-        up.wait_recv()
+        await_bytes(cg_v.at[pl.ds(0, 32), :], halo_sem.at[1])
     cg = cg_v[...].astype(F32)
     taps = taps_v[...].astype(F32)
     row = lax.broadcasted_iota(jnp.int32, (TOK, CH), 0)
@@ -572,10 +569,9 @@
 
     await_bytes(r_v.at[:, pl.ds(0, 15 * TOK // TP), :], za_send.at[0])
     to_partner.wait_send()
-    await_bytes(m0_v, m0_sem.at[Y])
+    await_bytes(m0_v, m0_sem.at[0])
     await_bytes(rf_v.at[pl.ds(0, 2)], rf_send.at[0])
-    down.wait_send()
-    up.wait_send()
+    await_bytes(cg_v.at[pl.ds(0, 32), :], halo_sem.at[0])
     await_bytes(rt_v.at[pl.ds(0, SP - 1)], rt_send.at[0])
 
 
@@ -623,9 +619,9 @@
             vm((SLOTS, CH), BF), vm(act, BF), vm(act, BF), vm(act, BF), vm(act, BF),
             vm((TP,) + act, BF), vm(act, BF), vm((16, CH), BF), vm((16, CH), BF),
             vm((C, Z, Y) + act, BF), vm((TP, Y, C, ROWS, TOK), BF), vm((SP, ROWS, TOK), BF),
-            dma((9,)), dma((2,)), dma((2,)), dma((Z + 1,)), dma((Z,)), dma((1,)), dma((Z,)),
-            dma((1,)), dma((Z,)), dma((2,)), dma((2,)), dma((2,)), dma((Y + 1,)), dma((1,)), dma((2, Y)),
-            dma((4,)), dma((1,)), dma((4,)), dma((2,)), dma((1,)), dma((Z,)),
+            dma((9,)), dma((2,)), dma((2,)), dma((Z + 1,)), dma((2,)), dma((1,)), dma((2,)),
+            dma((1,)), dma((Z,)), dma((2,)), dma((2,)), dma((2,)), dma((1,)), dma((1,)), dma((Y,)),
+            dma((2,)), dma((1,)), dma((4,)), dma((2,)), dma((1,)), dma((Z,)),
         ],
         compiler_params=pltpu.CompilerParams(
             collective_id=0, has_side_effects=True, vmem_limit_bytes=52428800

time: 61.5 us -> 61.3 us (level)
  Pallas kernels: 60.5 us -> 59.7 us
    pallas_call x1, Pallas kernels: 56.7 us -> 55.9 us  [per_device(): pl.pallas_call(layer_kernel, in_specs=[hbm] * 13, out_specs=[vmem] * 8, o...]
where the time goes in v5:
time: 61.3 us; the launch traced here: 60.4 us
  Pallas kernels  59.7 us (97%)
  between operations  0.65 us (1%)
    pallas_call x1, Pallas kernels, per_device(): pl.pallas_call(layer_kernel, in_specs=[hbm] * 13, out_specs=[vmem] * 8, o...  55.9 us
    pallas_call x1, Pallas kernels, per_device(): pl.pallas_call(flush_kernel, in_specs=[vmem] * 8, out_specs=[hbm] * 8, ou...  3.87 us

profile of v5, /device:TPU:0, one launch (start us, length us, event | category | flops | bytes accessed | tf_op | source)
XLA Modules:
  0.0 60.4 jit_solution(1627973106976129619)
XLA Ops:
  0.6 55.9 %shard_map.188 = (bf16[128,512]{1,0:T(8,128)(2,1)S(1)}, bf16[128,512]{1,0:T(8,128)(2,1)S(1)}, bf16[128,512]{1,0:T(8,128)(2,1)S(1)}, bf16[128,512]{1,0:T(8,128)(2...) custom-call(s32[2,128]{1,0:T(2,128)} %bitcast.13, ...), custom_call_target="tpu_custom_call" | custom-call | tf_op jit(solution)/shard_map/pallas_call | solution.py:606
  56.5 3.9 %shard_map.189 = (bf16[128,512]{1,0:T(8,128)(2,1)}, bf16[128,512]{1,0:T(8,128)(2,1)}, bf16[128,512]{1,0:T(8,128)(2,1)}, bf16[128,512]{1,0:T(8,128)(2,1)}, f32[64...) custom-call(bf16[128,512]{1,0:T(8,128)(2,1)S(1)} %get-tuple-element.24.refs_0_, ...), custom_call_target="tpu_custom_call" | custom-call | tf_op jit(solution)/shard_map/pallas_call | solution.py:633

commit v6 on v5

--- a/solution.py
+++ b/solution.py
@@ -283,10 +283,10 @@
     scatter(out2_v, 2, 1, recv2_sem, (2, 0))
     forward(1)
     hidden_tile(2)
+    forward(2)
+    forward(3)
     spread(1)
     scatter(out2_v, 2, 1, recv2_sem, (1, 3))
-    forward(2)
-    forward(3)
     await_bytes(dw_v, ld_sem.at[6])
 
     def give_back(src_ref, dst_ref, which, dzs):

time: 61.3 us -> 61 us (level)
  no operation moved by 1% of the time
where the time goes in v6:
time: 61 us; the launch traced here: 60.4 us
  Pallas kernels  59.7 us (98%)
  between operations  0.65 us (1%)
    pallas_call x1, Pallas kernels, per_device(): pl.pallas_call(layer_kernel, in_specs=[hbm] * 13, out_specs=[vmem] * 8, o...  55.9 us
    pallas_call x1, Pallas kernels, per_device(): pl.pallas_call(flush_kernel, in_specs=[vmem] * 8, out_specs=[hbm] * 8, ou...  3.87 us

profile of v6, /device:TPU:0, one launch (start us, length us, event | category | flops | bytes accessed | tf_op | source)
XLA Modules:
  0.0 60.4 jit_solution(3399901399814688919)
XLA Ops:
  0.6 55.9 %shard_map.188 = (bf16[128,512]{1,0:T(8,128)(2,1)S(1)}, bf16[128,512]{1,0:T(8,128)(2,1)S(1)}, bf16[128,512]{1,0:T(8,128)(2,1)S(1)}, bf16[128,512]{1,0:T(8,128)(2...) custom-call(s32[2,128]{1,0:T(2,128)} %bitcast.13, ...), custom_call_target="tpu_custom_call" | custom-call | tf_op jit(solution)/shard_map/pallas_call | solution.py:606
  56.5 3.9 %shard_map.189 = (bf16[128,512]{1,0:T(8,128)(2,1)}, bf16[128,512]{1,0:T(8,128)(2,1)}, bf16[128,512]{1,0:T(8,128)(2,1)}, bf16[128,512]{1,0:T(8,128)(2,1)}, f32[64...) custom-call(bf16[128,512]{1,0:T(8,128)(2,1)S(1)} %get-tuple-element.24.refs_0_, ...), custom_call_target="tpu_custom_call" | custom-call | tf_op jit(solution)/shard_map/pallas_call | solution.py:633
